TPU v7x, 1024 devices: a whole 4x8x16 slice. The times are simulated.
1024 devices in a mesh: sp: 128 (over z, y), tp: 8 (over x, core).
Axes of the slice: x: 4, y: 8, z: 16, core: 2. Of those that a mesh axis runs over, the one named last changes fastest.
Arguments:
- latent: bfloat16 [32768, 2048], P('sp'), may hold values from -6 to 6
- context: bfloat16 [512, 2048], P('sp'), may hold values from -6 to 6
- condition: float32 [2048], P('sp'), may hold values from -6 to 6
- ctx_condition: float32 [2048], P('sp'), may hold values from -6 to 6
- shift_weight: bfloat16 [2048, 2048], P('sp', 'tp'), may hold values from -0.125 to 0.125
- scale_weight: bfloat16 [2048, 2048], P('sp', 'tp'), may hold values from -0.125 to 0.125
- gate_weight: bfloat16 [2048, 2048], P('sp', 'tp'), may hold values from -0.125 to 0.125
- norm_gain: float32 [2048], replicated, may hold values from 0.1 to 1.9
- query_weight: bfloat16 [2048, 1024], P(None, 'tp'), may hold values from -0.125 to 0.125
- key_weight: bfloat16 [2048, 1024], P(None, 'tp'), may hold values from -0.125 to 0.125
- value_weight: bfloat16 [2048, 1024], P(None, 'tp'), may hold values from -0.125 to 0.125
- query_gain: float32 [64], replicated, may hold values from 0.6 to 6.5
- key_gain: float32 [64], replicated, may hold values from 0.6 to 6.5
- offset_bias: float32 [16, 15, 31], P('tp'), may hold values from 1 to 3
- out_weight: bfloat16 [1024, 2048], P('tp'), may hold values from -0.75 to 0.75
Outputs:
- mixed_rows: bfloat16 [32768, 2048], P('sp')
All inputs are finite; a program needn't handle non-finite values.
Results may differ from a plain program's by a relative error of at most 0.01405.
The roundings to bfloat16 on the way count: a program that leaves them out, or rounds other values in their place, can miss the bound.
Values may be sent and summed in bfloat16 or wider, within the bound.
A program may use at most 64 MiB of HBM per device.

v0:
```python
import jax
import jax.numpy as jnp
from jax import lax
from jax.sharding import Mesh
from jax.sharding import PartitionSpec as P

HEAD_DIM = 64
GRID_W = 64
WIN_ROWS = 8
WIN_COLS = 16
SP = ("sp_0", "sp_1")


EPS = 1e-06


def by_axis(x, axes):
    for axis in axes:
        x = lax.psum(x, axis)
    return x


def in_one_piece(arrays, axis, dim, along):
    ends, at = ([], 0)
    for a in arrays[:-1]:
        at += a.shape[along]
        ends.append(at)
    both = jnp.concatenate(arrays, axis=along)
    return tuple(jnp.split(lax.all_gather(both, axis, axis=dim, tiled=True), ends, axis=along))


def in_order(tiles, dim):
    tiles = jnp.moveaxis(tiles, 0, dim)
    dims = tiles.shape
    return tiles.reshape(*dims[:dim], dims[dim] * dims[dim + 1], *dims[dim + 2 :])


def all_blocks(x, axes, sequence):
    tiles = x[None]
    for k in sequence:
        tiles = lax.all_gather(tiles, axes[k], axis=0, tiled=True)
    held = [lax.axis_size(axes[k]) for k in reversed(sequence)]
    tiles = tiles.reshape(*held, *x.shape)
    turned = sorted(range(len(sequence)), key=lambda place: sequence[len(sequence) - 1 - place])
    return tiles.transpose(*turned, *range(len(sequence), tiles.ndim)).reshape(-1, *x.shape)


def whole_of(x, axes, sequence, dim):
    return in_order(all_blocks(x, axes, sequence), dim)


def extended(x, sides, width):
    for axis, dim in sides:
        count, length = (lax.axis_size(axis), x.shape[dim])
        up = [(i, (i + 1) % count) for i in range(count - 1)]
        down = [(j, i) for i, j in up]
        last = lax.slice_in_dim(x, length - width, length, axis=dim)
        initial = lax.slice_in_dim(x, 0, width, axis=dim)
        before = lax.ppermute(last, axis, up)
        after = lax.ppermute(initial, axis, down)
        x = jnp.concatenate([before, x, after], axis=dim)
    return x


def total_of_pieces(x, axis):
    tiles = lax.all_gather(x, axis).astype(jnp.float32)
    return tiles.sum(axis=0)


def modulate(rows_in, norm_gain, shift_vec, scale_vec):
    values = rows_in.astype(jnp.float32)
    normed = values * lax.rsqrt(jnp.mean(values * values, axis=-1, keepdims=True) + EPS)
    return (normed * norm_gain * (1.0 + scale_vec) + shift_vec).astype(jnp.bfloat16)


def head_norm(projected, head_gain):
    row_count = projected.shape[0]
    split_heads = projected.reshape(row_count, -1, head_gain.shape[0])
    normed = split_heads * lax.rsqrt(
        jnp.mean(split_heads * split_heads, axis=-1, keepdims=True) + EPS
    )
    return (normed * head_gain).astype(jnp.bfloat16).reshape(row_count, -1)


def per_device(
    latent,
    context,
    condition,
    ctx_condition,
    shift_weight,
    scale_weight,
    gate_weight,
    norm_gain,
    query_weight,
    key_weight,
    value_weight,
    query_gain,
    key_gain,
    offset_bias,
    out_weight,
):
    activations = jax.nn.silu(jnp.stack([condition, ctx_condition])).astype(jnp.bfloat16)
    part_shift = jnp.dot(activations, shift_weight, preferred_element_type=jnp.float32)
    part_scale = jnp.dot(activations, scale_weight, preferred_element_type=jnp.float32)
    part_gate = jnp.dot(activations[:1], gate_weight, preferred_element_type=jnp.float32)
    summed = (by_axis(part_shift, SP), by_axis(part_scale, SP), by_axis(part_gate, SP))
    shift_vec, scale_vec, gate_vec = in_one_piece((summed[0], summed[1], summed[2]), "tp", 1, 0)
    hidden = modulate(latent, norm_gain, shift_vec[0], scale_vec[0])
    queries = head_norm(
        jnp.dot(hidden, query_weight, preferred_element_type=jnp.float32), query_gain
    )
    keys_lat = head_norm(jnp.dot(hidden, key_weight, preferred_element_type=jnp.float32), key_gain)
    values_lat = jnp.dot(hidden, value_weight, preferred_element_type=jnp.float32).astype(
        jnp.bfloat16
    )
    ctx_hidden = modulate(context, norm_gain, shift_vec[1], scale_vec[1])
    ctx_keys = head_norm(
        jnp.dot(ctx_hidden, key_weight, preferred_element_type=jnp.float32), key_gain
    )
    ctx_values = jnp.dot(ctx_hidden, value_weight, preferred_element_type=jnp.float32).astype(
        jnp.bfloat16
    )
    ctx_pairs = whole_of(jnp.concatenate([ctx_keys, ctx_values], axis=1), SP, (0, 1), 0)
    col_width = keys_lat.shape[1]
    heads_dev = col_width // HEAD_DIM
    local_rows = keys_lat.shape[0] // GRID_W
    halo_rows = WIN_ROWS // 2
    window_keys = WIN_ROWS * GRID_W
    key_value = jnp.concatenate([keys_lat, values_lat], axis=1).reshape(
        local_rows, GRID_W, 2 * col_width
    )
    padded = extended(key_value, ((SP, 0),), halo_rows)
    first_row = lax.axis_index(SP) * local_rows
    total_rows = local_rows * lax.axis_size(SP)
    global_rows = first_row + jnp.arange(local_rows, dtype=jnp.int32)
    band_start = jnp.clip(global_rows - halo_rows, 0, total_rows - WIN_ROWS)
    band_global = band_start[:, None] + jnp.arange(WIN_ROWS, dtype=jnp.int32)[None, :]
    banded = jnp.take(padded, band_global - first_row + halo_rows, axis=0)
    key_band = banded[..., :col_width].reshape(local_rows, window_keys, heads_dev, HEAD_DIM)
    value_band = banded[..., col_width:].reshape(local_rows, window_keys, heads_dev, HEAD_DIM)
    row_steps = band_global - global_rows[:, None] + WIN_ROWS - 1
    row_hot = (
        row_steps[:, :, None] == jnp.arange(2 * WIN_ROWS - 1, dtype=jnp.int32)[None, None, :]
    ).astype(jnp.float32)
    column_ids = jnp.arange(GRID_W, dtype=jnp.int32)
    col_steps = (
        jnp.clip(column_ids[None, :] - column_ids[:, None], 1 - WIN_COLS, WIN_COLS - 1)
        + WIN_COLS
        - 1
    )
    col_hot = (
        col_steps[:, :, None] == jnp.arange(2 * WIN_COLS - 1, dtype=jnp.int32)[None, None, :]
    ).astype(jnp.float32)
    col_start = jnp.clip(column_ids - WIN_COLS // 2, 0, GRID_W - WIN_COLS)
    col_open = (column_ids[None, :] >= col_start[:, None]) & (
        column_ids[None, :] < col_start[:, None] + WIN_COLS
    )
    col_table = jnp.einsum("hab,qkb->haqk", offset_bias, col_hot, precision=lax.Precision.HIGHEST)
    col_table = jnp.where(col_open[None, None, :, :], col_table, -jnp.inf)
    offset_terms = jnp.einsum(
        "rja,haqk->hrqjk",
        row_hot,
        jnp.where(col_open[None, None], col_table, 0.0),
        precision=lax.Precision.HIGHEST,
    )
    offset_terms = jnp.where(col_open[None, None, :, None, :], offset_terms, -jnp.inf)
    offset_terms = offset_terms.reshape(heads_dev, local_rows, GRID_W, window_keys)
    score_scale = HEAD_DIM ** (-0.5)
    q_grid = queries.reshape(local_rows, GRID_W, heads_dev, HEAD_DIM)
    scores = (
        jnp.einsum("rqhd,rnhd->hrqn", q_grid, key_band, preferred_element_type=jnp.float32)
        * score_scale
        + offset_terms
    )
    ctx_count = ctx_pairs.shape[0]
    ctx_keys_all = ctx_pairs[:, :col_width].reshape(ctx_count, heads_dev, HEAD_DIM)
    ctx_values_all = ctx_pairs[:, col_width:].reshape(ctx_count, heads_dev, HEAD_DIM)
    ctx_scores = (
        jnp.einsum("rqhd,nhd->hrqn", q_grid, ctx_keys_all, preferred_element_type=jnp.float32)
        * score_scale
    )
    row_max = jnp.maximum(jnp.max(scores, axis=3), jnp.max(ctx_scores, axis=3))
    local_exp = jnp.exp(scores - row_max[..., None])
    ctx_exp = jnp.exp(ctx_scores - row_max[..., None])
    denominator = jnp.sum(local_exp, axis=3) + jnp.sum(ctx_exp, axis=3)
    local_weights = (local_exp / denominator[..., None]).astype(jnp.bfloat16)
    ctx_weights = (ctx_exp / denominator[..., None]).astype(jnp.bfloat16)
    combined = jnp.einsum(
        "hrqn,rnhd->rqhd", local_weights, value_band, preferred_element_type=jnp.float32
    ) + jnp.einsum(
        "hrqn,nhd->rqhd", ctx_weights, ctx_values_all, preferred_element_type=jnp.float32
    )
    attended = combined.astype(jnp.bfloat16).reshape(local_rows * GRID_W, col_width)
    partial_value = jnp.dot(attended, out_weight, preferred_element_type=jnp.float32)
    branch = total_of_pieces(partial_value.astype(jnp.bfloat16), "tp").astype(jnp.float32)
    return (latent.astype(jnp.float32) + gate_vec[0] * branch).astype(jnp.bfloat16)


def solution(mesh):
    split = Mesh(mesh.devices.reshape(16, 8, mesh.shape["tp"]), ("sp_0", "sp_1", "tp"))
    placed = (
        P(SP, None),
        P(SP, None),
        P(SP),
        P(SP),
        P(SP, "tp"),
        P(SP, "tp"),
        P(SP, "tp"),
        P(),
        P(None, "tp"),
        P(None, "tp"),
        P(None, "tp"),
        P(),
        P(),
        P("tp", None, None),
        P("tp", None),
    )
    return jax.shard_map(
        per_device, mesh=split, in_specs=placed, out_specs=P(SP, None), check_vma=False
    )
```

profile of v0, /device:TPU:1, one launch (start us, length us, event | category | flops | bytes accessed | tf_op | source)
XLA Modules:
  0.0 236.5 jit_solution(11539275351324366267)
XLA Ops:
  6.5 0.7 mul.182
  7.4 1.5 fusion
  8.9 0.7 fusion.30
  9.6 0.8 fusion.31
  10.5 0.8 fusion.45
  11.3 0.8 fusion.44
  12.1 37.5 %all-reduce = (f32[1,256]{1,0:T(1,128)S(1)}, f32[2,256]{1,0:T(2,128)S(1)}, f32[2,256]{1,0:T(2,128)S(1)}) all-reduce(f32[1,256]{1,0:T(1,128)S(1)} %fusion.31, f32[2,256]{1,0:T(2,128)S(1)} %fusion.45, f32[2,256]{1,0:T(2,128)S(1)} %fusion.44), channel_id=1, replica_groups=mesh['sp_0'=16,'sp_1'=8,'tp'=8] {'sp_0'}, use_global_device_ids=true, to_apply=%region_4.5 | all-reduce | flops 1280 | bytes 10240 | tf_op jit(solution)/shard_map/psum | solution.py:19
  49.6 14.1 %all-reduce.1 = (f32[1,256]{1,0:T(1,128)S(1)}, f32[2,256]{1,0:T(2,128)S(1)}, f32[2,256]{1,0:T(2,128)S(1)}) all-reduce(f32[1,256]{1,0:T(1,128)S(1)} %get-tuple-element.7, f32[2,256]{1,0:T(2,128)S(1)} %get-tuple-element.8, f32[2,256]{1,0:T(2,128)S(1)} %get-tuple-element.9), channel_id=1, replica_groups=mesh['sp_0'=16,'sp_1'=8,'tp'=8] {'sp_1'}, use_global_device_ids=true, to_apply=%region_5.6 | all-reduce | flops 1280 | bytes 10240 | tf_op jit(solution)/shard_map/psum | solution.py:19
  63.8 24.5 %all_gather.15 = f32[5,2048]{1,0:T(8,128)S(1)} all-gather(f32[5,256]{1,0:T(8,128)S(1)} %pad_maximum_fusion.2), channel_id=1, replica_groups=mesh['sp_0'=16,'sp_1'=8,'tp'=8] {'tp'}, dimensions={1}, use_global_device_ids=true | all-gather | bytes 46080 | tf_op jit(solution)/shard_map/all_gather | solution.py:29
  88.2 1.7 fusion.4
  91.1 1.3 collective-permute-start.1
  92.4 4.6 %collective-permute-start = (bf16[4,64,256]{2,1,0:T(8,128)(2,1)S(1)}, bf16[4,64,256]{2,1,0:T(8,128)(2,1)}, u32[]{:S(2)}, u32[]{:S(2)}) collective-permute-start(bf16[4,64,256]{2,1,0:T(8,128)(2,1)S(1)} %pad_maximum_fusion.1), channel_id=1, source_target_pairs={{0,8},{8,16},{16,24},{24,32},{32,40},{40,48},{48,56},{56,64},{64,7... | collective-permute-start | bytes 393224 | tf_op jit(solution)/shard_map/ppermute | solution.py:59
  98.3 19.6 %all-gather.2 = bf16[16,4,256]{2,1,0:T(4,128)(2,1)S(1)} all-gather(bf16[1,4,256]{2,1,0:T(4,128)(2,1)S(1)} %maximum_bitcast_fusion), channel_id=2, replica_groups=mesh['sp_0'=16,'sp_1'=8,'tp'=8] {'sp_0'}, dimensions={0}, use_global_device_ids=true | all-gather | bytes 34816 | tf_op jit(solution)/shard_map/all_gather | solution.py:41
  117.9 19.0 %all_gather.17 = bf16[128,4,256]{2,1,0:T(4,128)(2,1)S(1)} all-gather(bf16[16,4,256]{2,1,0:T(4,128)(2,1)S(1)} %all-gather.2), channel_id=1, replica_groups=mesh['sp_0'=16,'sp_1'=8,'tp'=8] {'sp_1'}, dimensions={0}, use_global_device_ids=true | all-gather | bytes 294912 | tf_op jit(solution)/shard_map/all_gather | solution.py:41
  137.3 0.5 bitcast_reduce_fusion
  138.3 0.6 fusion.8
  139.0 2.4 %select_bitcast_fusion = f32[2,4,64,8,64]{4,3,1,2,0:T(8,128)} fusion(f32[2,15,64,64,1]{3,1,4,2,0:T(8,128)S(1)} %fusion.8, pred[64,64]{1,0:T(8,128)(4,1)S(1)} %fusion.25, s32[4,8]{1,0:T(4,128)S(1)} %subtract_add_fusion), kind=kOutput, calls=%fused_computation.12 | convolution fusion | flops 47448544 | bytes 1544320 | tf_op jit(solution)/shard_map/rja,haqk->hrqjk/dot_general | solution.py:160
  141.8 0.7 compare_and_fusion
  142.7 2.1 reshape.342
  144.8 0.6 pad_clamp_fusion
  145.4 0.7 copy-done.6
  146.0 1.0 pad_maximum_fusion
  147.0 1.7 gather_fusion
  148.7 1.4 broadcast_select_fusion
  150.1 1.1 fusion.37
  151.2 1.4 reshape.341
  152.6 1.9 fusion.42
  155.5 0.6 copy-done.2
  157.6 1.4 convolution_convert_fusion
  159.0 63.8 %all-gather.5.cloned.1.call-done = bf16[2048,2048]{1,0:T(8,128)(2,1)} async-done(((bf16[256,2048]{1,0:T(8,128)(2,1)}), bf16[2048,2048]{1,0:T(8,128)(2,1)}) %all-gather.5.cloned.1.call-update) | async-done | bytes 8388624 | tf_op jit(solution)/shard_map/all_gather | solution.py:66
  222.9 5.5 %convert_reduce_fusion = f32[256,2048]{1,0:T(8,128)S(1)} fusion(bf16[8,256,2048]{2,1,0:T(8,128)(2,1)} %bitcast.93), kind=kLoop, calls=%fused_computation.1 | loop fusion | flops 7864320 | bytes 10485760 | tf_op jit(solution)/shard_map/reduce_sum | solution.py:67
  228.4 1.3 fusion.5
  (75 shorter events, 6.3 us)
Async XLA Ops:
  6.5 151.1 %copy-start = (bf16[128,2048]{1,0:T(8,128)(2,1)S(1)}, bf16[128,2048]{1,0:T(8,128)(2,1)}, u32[]{:S(2)}) copy-start(bf16[128,2048]{1,0:T(8,128)(2,1)} %param.29) | copy-start | bytes 1572868
  6.5 83.4 %copy-start.3 = (bf16[2048,128]{1,0:T(8,128)(2,1)S(1)}, bf16[2048,128]{1,0:T(8,128)(2,1)}, u32[]{:S(2)}) copy-start(bf16[2048,128]{1,0:T(8,128)(2,1)} %param.25) | copy-start | bytes 1572868
  6.5 216.3 %all-gather.5.cloned.1.call-start = ((), (), s32[]{:S(2)}) async-start(), calls=%async_computation | async-start | bytes 9437184 | tf_op jit(solution)/shard_map/all_gather | solution.py:66
  8.9 81.5 %copy-start.4 = (bf16[2048,128]{1,0:T(8,128)(2,1)S(1)}, bf16[2048,128]{1,0:T(8,128)(2,1)}, u32[]{:S(2)}) copy-start(bf16[2048,128]{1,0:T(8,128)(2,1)} %param.24) | copy-start | bytes 1572868
  89.9 7.2 %copy-start.7 = (bf16[4,2048]{1,0:T(4,128)(2,1)S(1)}, bf16[4,2048]{1,0:T(4,128)(2,1)}, u32[]{:S(2)}) copy-start(bf16[4,2048]{1,0:T(4,128)(2,1)} %param.16) | copy-start | bytes 49156
  90.0 7.3 %copy-start.8 = (f32[2048]{0:T(1024)S(1)}, f32[2048]{0:T(1024)}, u32[]{:S(2)}) copy-start(f32[2048]{0:T(1024)} %param.22) | copy-start | bytes 24580
  91.1 54.2 %collective-permute-start.1 = (bf16[4,64,256]{2,1,0:T(8,128)(2,1)S(1)}, bf16[4,64,256]{2,1,0:T(8,128)(2,1)S(1)}, u32[]{:S(2)}, u32[]{:S(2)}) collective-permute-start(bf16[4,64,256]{2,1,0:T(8,128)(2,1)S(1)} %pad_maximum_fusion.1), channel_id=1, source_target_pairs={{8,0},{16,8},{24,16},{32,24},{40,32},{48,40},{56,48},{64,56},{72,6... | collective-permute-start | bytes 393224 | tf_op jit(solution)/shard_map/ppermute | solution.py:60
  92.4 53.6 %collective-permute-start = (bf16[4,64,256]{2,1,0:T(8,128)(2,1)S(1)}, bf16[4,64,256]{2,1,0:T(8,128)(2,1)}, u32[]{:S(2)}, u32[]{:S(2)}) collective-permute-start(bf16[4,64,256]{2,1,0:T(8,128)(2,1)S(1)} %pad_maximum_fusion.1), channel_id=1, source_target_pairs={{0,8},{8,16},{16,24},{24,32},{32,40},{40,48},{48,56},{56,64},{64,7... | collective-permute-start | bytes 393224 | tf_op jit(solution)/shard_map/ppermute | solution.py:59
  97.8 39.5 %copy-start.5 = (bf16[2048,128]{1,0:T(8,128)(2,1)S(1)}, bf16[2048,128]{1,0:T(8,128)(2,1)}, u32[]{:S(2)}) copy-start(bf16[2048,128]{1,0:T(8,128)(2,1)} %param.23) | copy-start | bytes 1572868
  137.1 1.2 copy-start.10
  138.3 3.1 %copy-start.9 = (f32[64]{0:T(128)S(1)}, f32[64]{0:T(128)}, u32[]{:S(2)}) copy-start(f32[64]{0:T(128)} %param.26) | copy-start | bytes 772
  145.4 0.7 copy-start.6
  155.1 1.0 copy-start.2
  222.9 5.5 %copy-start.1 = (bf16[256,2048]{1,0:T(8,128)(2,1)S(1)}, bf16[256,2048]{1,0:T(8,128)(2,1)}, u32[]{:S(2)}) copy-start(bf16[256,2048]{1,0:T(8,128)(2,1)} %param.15) | copy-start | bytes 3145732
Sparse Core Ops, SparseCore 0:
  159.1 63.6 all-gather.4
where the time goes:
time: 237 us
  blocking collectives  115 us (49%)
  waiting for transfers between devices  63.9 us (27%)
  other arithmetic  15.9 us (7%)
  between operations  13.8 us (6%)
  matrix products  11.9 us (5%)
  local copies, waits for them, and re-layouts  10.3 us (4%)
  starting transfers between devices  5.94 us (3%)
    all_gather x1, waiting for transfers between devices, total_of_pieces(): tiles = lax.all_gather(x, axis).astype(jnp.float32)  63.8 us
    psum x2, blocking collectives, by_axis(): x = lax.psum(x, axis)  51.6 us
    all_gather x2, blocking collectives, all_blocks(): tiles = lax.all_gather(tiles, axes[k], axis=0, tiled=True)  38.6 us
    all_gather x1, blocking collectives, in_one_piece(): lax.all_gather(both, axis, axis=dim, tiled=True)  24.5 us
    reduce_sum x1, other arithmetic, total_of_pieces(): return tiles.sum(axis=0)  5.48 us
  transfers between devices with their start and end apart: 3, of which 1 were waited for; matrix products, arithmetic and copies ran while one was open for 4% of the time, Pallas kernels for 0%

commit v1 on v0

v1 whole, which is shorter than its diff:
```python
import jax
import jax.numpy as jnp
from jax import lax
from jax.experimental import pallas as pl
from jax.experimental.pallas import tpu as pltpu
from jax.sharding import PartitionSpec as P

MESH = pl.DeviceIdType.MESH
EPS = 1e-06
Z, Y, TP = 16, 8, 8
SP = Z * Y
D = 2048
F = D // TP
TOK = 256
COLS = 64
ROWS = 4
HD = 64
NEG = float("-inf")


def rem(a, n):
    return lax.rem(a, jnp.int32(n))


def head_norm(p, gain2):
    lane = lax.broadcasted_iota(jnp.int32, p.shape, 1)
    left = lane < HD
    sq = p * p
    s0 = jnp.sum(jnp.where(left, sq, 0.0), axis=1, keepdims=True)
    s1 = jnp.sum(jnp.where(left, 0.0, sq), axis=1, keepdims=True)
    r0 = lax.rsqrt(s0 * (1.0 / HD) + EPS)
    r1 = lax.rsqrt(s1 * (1.0 / HD) + EPS)
    return p * jnp.where(left, r0, r1) * gain2


def kernel(
    latent, context, cond, cctx, shw, scw, gw, gain, wq, wk, wv, qg, kg, bias, outw,
    out,
    part, mody, zpart, modz, modf,
    cbuf, cf, ckv,
    hbuf, xn, hid,
    wqv, wkvv, wfull, latv,
    tbl, kpad, vpad, q2, ew, attb, outv,
    loc_sem, out_sem,
    ys, yr, zs, zr, ts, tr,
    czs, czr, cts, ctr, cys, cyr,
    hs, hr, hps, hpr,
    ws, wr, wps, wpr,
    as_, ar,
):
    sp = lax.axis_index("sp")
    tp = lax.axis_index("tp")
    y = rem(sp, Y)
    z = lax.div(sp, jnp.int32(Y))
    c = rem(tp, 2)
    partner = tp + 1 - 2 * c
    up = rem(sp + 1, SP)
    down = rem(sp + SP - 1, SP)
    right = rem(tp + 2, TP)
    left = rem(tp + TP - 2, TP)
    far = rem(tp + 4, TP)

    def y_peer(k):
        return {"sp": z * Y + rem(y + k, Y), "tp": tp}

    def z_peer(k):
        return {"sp": rem(z + k, Z) * Y + y, "tp": tp}

    def t_peer(k):
        return {"sp": sp, "tp": rem(tp + k, TP)}

    def at(s, t):
        return {"sp": s, "tp": t}

    def remote(src, dst, s, r, dev):
        return pltpu.make_async_remote_copy(
            src_ref=src, dst_ref=dst, send_sem=s, recv_sem=r, device_id=dev, device_id_type=MESH
        )

    sends = []

    def send(src, dst, s, r, dev):
        d = remote(src, dst, s, r, dev)
        d.start()
        sends.append(d)
        return d

    barrier = pltpu.get_barrier_semaphore()
    peers = [z_peer(k) for k in (8, 7, 9, 6, 10, 5, 11, 4, 12, 3, 13, 2, 14, 1, 15)]
    peers += [y_peer(k) for k in range(1, Y)]
    peers += [t_peer(k) for k in range(1, TP)]
    peers += [at(up, tp), at(down, tp)]
    for p in peers:
        pl.semaphore_signal(barrier, inc=1, device_id=p, device_id_type=MESH)

    ctx_col = pl.multiple_of(tp * F, F)
    own_c = pltpu.make_async_copy(context.at[:, pl.ds(ctx_col, F)], cbuf.at[tp, z], loc_sem.at[0])
    own_l = pltpu.make_async_copy(latent, latv, loc_sem.at[1])
    own_q = pltpu.make_async_copy(wq, wqv, loc_sem.at[2])
    own_k = pltpu.make_async_copy(wk, wkvv.at[:, pl.ds(0, 128)], loc_sem.at[3])
    own_v = pltpu.make_async_copy(wv, wkvv.at[:, pl.ds(128, 128)], loc_sem.at[4])
    own_w = pltpu.make_async_copy(outw, wfull.at[tp], loc_sem.at[5])
    own_c.start()
    own_l.start()
    own_w.start()
    own_q.start()
    own_k.start()
    own_v.start()

    row8 = lax.broadcasted_iota(jnp.int32, (8, 16), 0)
    pre = jnp.where(row8 == 0, jnp.broadcast_to(cond[...], (8, 16)), jnp.broadcast_to(cctx[...], (8, 16)))
    act = (pre / (1.0 + jnp.exp(-pre))).astype(jnp.bfloat16)
    p_sh = jnp.dot(act, shw[...], preferred_element_type=jnp.float32)
    p_sc = jnp.dot(act, scw[...], preferred_element_type=jnp.float32)
    p_g = jnp.dot(act, gw[...], preferred_element_type=jnp.float32)
    part[0:2, :] = p_sh[0:2]
    part[2:4, :] = p_sc[0:2]
    part[4:5, :] = p_g[0:1]

    pl.semaphore_wait(barrier, len(peers))

    for k in (4, 3, 5, 2, 6, 1, 7):
        send(part, mody.at[k - 1], ys.at[k - 1], yr.at[k - 1], y_peer(k))
    own_c.wait()
    for k in (8, 7, 9, 6, 10, 5, 11, 4, 12, 3, 13, 2, 14, 1, 15):
        send(cbuf.at[tp, z], cbuf.at[tp, z], czs.at[k - 1], czr.at[k - 1], z_peer(k))
    own_l.wait()
    own_w.wait()
    half = pl.ds(pl.multiple_of(c * 128, 128), 128)
    halo_up = send(latv.at[half], hbuf.at[0, half], hs.at[0], hr.at[0], at(up, tp))
    halo_dn = send(latv.at[half], hbuf.at[1, half], hs.at[1], hr.at[1], at(down, tp))
    w_right = send(wfull.at[tp], wfull.at[tp], ws.at[0], wr.at[0], at(sp, right))
    w_left = send(wfull.at[tp], wfull.at[tp], ws.at[1], wr.at[1], at(sp, left))
    send(wfull.at[tp], wfull.at[tp], wps.at[0], wpr.at[0], at(sp, partner))

    tq = lax.broadcasted_iota(jnp.int32, (COLS, 128), 0)
    tl = lax.broadcasted_iota(jnp.int32, (COLS, 128), 1)
    tk = jnp.where(tl < COLS, tl, tl - COLS)
    diff = tk - tq + 15
    c0 = jnp.clip(tq - 8, 0, 48)
    is_open = (tk >= c0) & (tk < c0 + 16)
    first = lax.broadcasted_iota(jnp.int32, (1, 128), 1) < COLS

    def table_step(n, carry):
        h = lax.div(n, jnp.int32(14))
        a = rem(n, 14)
        val = jnp.full((COLS, 128), NEG, jnp.float32)
        for dd in range(31):
            v = jnp.where(first, bias[h, a, dd], bias[h, a + 1, dd])
            val = jnp.where(diff == dd, jnp.broadcast_to(v, (COLS, 128)), val)
        tbl[h, a] = jnp.where(is_open, val, NEG)
        return carry

    lax.fori_loop(0, 28, table_step, 0)

    def normed(load, store, rows, chunk):
        def step(n, carry):
            r = pl.ds(pl.multiple_of(n * chunk, chunk), chunk)
            v = load(r).astype(jnp.float32)
            ms = jnp.mean(v * v, axis=-1, keepdims=True)
            store(r, v * lax.rsqrt(ms + EPS) * gain[...])
            return carry

        lax.fori_loop(0, rows // chunk, step, 0)

    acc = part[...]
    for k in range(1, Y):
        remote(part, mody.at[k - 1], ys.at[k - 1], yr.at[k - 1], y_peer(k)).wait_recv()
        acc = acc + mody[k - 1]
    zpart[...] = acc
    for k in (8, 7, 9, 6, 10, 5, 11, 4, 12, 3, 13, 2, 14, 1, 15):
        send(zpart, modz.at[k - 1], zs.at[k - 1], zr.at[k - 1], z_peer(k))

    def store_own(r, v):
        xn[1, r, :] = v

    normed(lambda r: latv[r, :], store_own, TOK, 16)

    for k in range(1, Z):
        remote(cbuf.at[tp, z], cbuf.at[tp, z], czs.at[k - 1], czr.at[k - 1], z_peer(k)).wait_recv()
    for k in range(1, TP):
        send(cbuf.at[tp], cbuf.at[tp], cts.at[k - 1], ctr.at[k - 1], t_peer(k))

    acc = zpart[...]
    for k in range(1, Z):
        remote(zpart, modz.at[k - 1], zs.at[k - 1], zr.at[k - 1], z_peer(k)).wait_recv()
        acc = acc + modz[k - 1]
    modf[tp] = acc
    for k in range(1, TP):
        send(modf.at[tp], modf.at[tp], ts.at[k - 1], tr.at[k - 1], t_peer(k))

    halo_up.wait_recv()
    send(hbuf.at[0, half], hbuf.at[0, half], hps.at[0], hpr.at[0], at(sp, partner))
    halo_dn.wait_recv()
    send(hbuf.at[1, half], hbuf.at[1, half], hps.at[1], hpr.at[1], at(sp, partner))

    for k in range(1, TP):
        remote(cbuf.at[tp], cbuf.at[tp], cts.at[k - 1], ctr.at[k - 1], t_peer(k)).wait_recv()
    for zz in range(Z):
        for g in range(TP):
            cf[4 * zz : 4 * zz + 4, g * F : (g + 1) * F] = cbuf[g, zz].astype(jnp.float32)

    def store_ctx(r, v):
        cf[r, :] = v

    normed(lambda r: cf[r, :], store_ctx, 64, 16)

    for s in range(2):
        remote(hbuf.at[s, half], hbuf.at[s, half], hps.at[s], hpr.at[s], at(sp, partner)).wait_recv()

        def store_halo(r, v, s=s):
            xn[2 * s, r, :] = v

        normed(lambda r, s=s: hbuf[s, r, :], store_halo, TOK, 16)

    lo, hi = pl.ds(0, 64), pl.ds(64, 64)
    w_right.wait_recv()
    send(wfull.at[left, lo], wfull.at[left, lo], ws.at[2], wr.at[2], at(sp, right))
    send(wfull.at[left], wfull.at[left], wps.at[1], wpr.at[1], at(sp, partner))
    w_left.wait_recv()
    send(wfull.at[right, hi], wfull.at[right, hi], ws.at[3], wr.at[3], at(sp, left))
    send(wfull.at[right], wfull.at[right], wps.at[2], wpr.at[2], at(sp, partner))

    for k in range(1, TP):
        remote(modf.at[tp], modf.at[tp], ts.at[k - 1], tr.at[k - 1], t_peer(k)).wait_recv()

    own_k.wait()
    own_v.wait()
    own_q.wait()
    lane = lax.broadcasted_iota(jnp.int32, (1, 128), 1)
    qg2 = jnp.concatenate([qg[...], qg[...]], axis=1)
    kg2 = jnp.concatenate([kg[...], kg[...]], axis=1)

    for g in range(TP):
        gs = slice(g * F, (g + 1) * F)
        hid[0:64, gs] = (cf[:, gs] * (1.0 + modf[g, 3:4, :]) + modf[g, 1:2, :]).astype(jnp.bfloat16)
    kv = jnp.dot(hid[0:64, :], wkvv[...], preferred_element_type=jnp.float32)
    ckv[y, :, 0:128] = head_norm(kv[:, 0:128], kg2).astype(jnp.bfloat16)
    ckv[y, :, 128:256] = kv[:, 128:256].astype(jnp.bfloat16)
    for k in (4, 3, 5, 2, 6, 1, 7):
        send(ckv.at[y], ckv.at[y], cys.at[k - 1], cyr.at[k - 1], y_peer(k))

    for b in (1, 0, 2):
        def rows_step(n, carry, b=b):
            r = pl.ds(pl.multiple_of(n * 128, 128), 128)
            for g in range(TP):
                gs = slice(g * F, (g + 1) * F)
                hid[:, gs] = (xn[b, r, gs] * (1.0 + modf[g, 2:3, :]) + modf[g, 0:1, :]).astype(jnp.bfloat16)
            h = hid[...]
            kv = jnp.dot(h, wkvv[...], preferred_element_type=jnp.float32)
            kr = pl.ds(pl.multiple_of(b * TOK + n * 128, 128), 128)
            kpad[kr, :] = head_norm(kv[:, 0:128], kg2).astype(jnp.bfloat16)
            vpad[kr, :] = kv[:, 128:256].astype(jnp.bfloat16)
            if b == 1:
                q = jnp.dot(h, wqv[...], preferred_element_type=jnp.float32)
                q = (head_norm(q, qg2) * (HD**-0.5)).astype(jnp.bfloat16)
                zero = jnp.zeros_like(q)
                lf = jnp.broadcast_to(lane < HD, q.shape)
                q0 = jnp.where(lf, q, zero)
                q1 = jnp.where(lf, zero, q)
                for i in range(2):
                    q2[2 * n + i, 0:64, :] = q0[i * 64 : (i + 1) * 64]
                    q2[2 * n + i, 64:128, :] = q1[i * 64 : (i + 1) * 64]
            return carry

        lax.fori_loop(0, 2, rows_step, 0)

    nt = (((1,), (1,)), ((), ()))
    at_first = sp == 0
    at_last = sp == SP - 1
    m_w, l_w, band = [], [], []
    for i in range(ROWS):
        start = jnp.where(at_first, 4, jnp.where(at_last, 0, i))
        off = jnp.where(at_first, 7 - i, 3 + jnp.where(at_last, -i, 0))
        rows = pl.ds(pl.multiple_of(start * COLS, COLS), 8 * COLS)
        band.append(rows)
        s = lax.dot_general(q2[i], kpad[rows, :], nt, preferred_element_type=jnp.float32)
        tiles = []
        for p in range(4):
            t = jnp.concatenate([tbl[0, off + 2 * p], tbl[1, off + 2 * p]], axis=0)
            tiles.append(s[:, p * 128 : (p + 1) * 128] + t)
        s = jnp.concatenate(tiles, axis=1)
        m = jnp.max(s, axis=1, keepdims=True)
        e = jnp.exp(s - m)
        ew[i] = e
        m_w.append(m)
        l_w.append(jnp.sum(e, axis=1, keepdims=True))

    remote(wfull.at[left, lo], wfull.at[far, lo], ws.at[2], wr.at[2], at(sp, right)).wait_recv()
    remote(wfull.at[right, hi], wfull.at[far, hi], ws.at[3], wr.at[3], at(sp, left)).wait_recv()
    send(wfull.at[far], wfull.at[far], wps.at[3], wpr.at[3], at(sp, partner))

    for k in range(1, Y):
        remote(ckv.at[y], ckv.at[y], cys.at[k - 1], cyr.at[k - 1], y_peer(k)).wait_recv()
    ck = ckv[:, :, 0:128].reshape(512, 128)
    cv = ckv[:, :, 128:256].reshape(512, 128)
    for i in range(ROWS):
        sc = lax.dot_general(q2[i], ck, nt, preferred_element_type=jnp.float32)
        m = jnp.maximum(m_w[i], jnp.max(sc, axis=1, keepdims=True))
        ec = jnp.exp(sc - m)
        fw = jnp.exp(m_w[i] - m)
        inv = 1.0 / (l_w[i] * fw + jnp.sum(ec, axis=1, keepdims=True))
        w_win = (ew[i] * (fw * inv)).astype(jnp.bfloat16)
        w_ctx = (ec * inv).astype(jnp.bfloat16)
        o = jnp.dot(w_win, vpad[band[i], :], preferred_element_type=jnp.float32) + jnp.dot(
            w_ctx, cv, preferred_element_type=jnp.float32
        )
        o = jnp.where(jnp.broadcast_to(lane < HD, (64, 128)), o[0:64], o[64:128])
        attb[tp, i * COLS : (i + 1) * COLS, :] = o.astype(jnp.bfloat16)
    for k in (4, 2, 6, 3, 5, 1, 7):
        send(attb.at[tp], attb.at[tp], as_.at[k - 1], ar.at[k - 1], t_peer(k))

    for k in range(1, TP):
        remote(attb.at[tp], attb.at[tp], as_.at[k - 1], ar.at[k - 1], t_peer(k)).wait_recv()
    for n in range(4):
        remote(wfull.at[tp], wfull.at[tp], wps.at[n], wpr.at[n], at(sp, partner)).wait_recv()

    def out_copy(n):
        cols = pl.ds(pl.multiple_of(n * F, F), F)
        return pltpu.make_async_copy(outv.at[:, cols], out.at[:, cols], out_sem.at[n])

    def proj_step(n, carry):
        cols = pl.ds(pl.multiple_of(n * F, F), F)
        acc = jnp.zeros((TOK, F), jnp.float32)
        for g in range(TP):
            t = jnp.dot(attb[g], wfull[g, :, cols], preferred_element_type=jnp.float32)
            acc = acc + t.astype(jnp.bfloat16).astype(jnp.float32)
        res = latv[:, cols].astype(jnp.float32) + modf[n, 4:5, :] * acc
        outv[:, cols] = res.astype(jnp.bfloat16)
        out_copy(n).start()
        return carry

    lax.fori_loop(0, TP, proj_step, 0)

    for d in sends:
        d.wait_send()
    for n in range(TP):
        out_copy(n).wait()


def per_device(latent, context, cond, cctx, shw, scw, gw, gain, wq, wk, wv, qg, kg, bias, outw):
    any_ = pl.BlockSpec(memory_space=pl.ANY)
    vm = pl.BlockSpec(memory_space=pltpu.VMEM)
    sm = pl.BlockSpec(memory_space=pltpu.SMEM)
    bf, f32 = jnp.bfloat16, jnp.float32
    dma = pltpu.SemaphoreType.DMA
    scratch = [
        pltpu.VMEM((5, F), f32),
        pltpu.VMEM((Y - 1, 5, F), f32),
        pltpu.VMEM((5, F), f32),
        pltpu.VMEM((Z - 1, 5, F), f32),
        pltpu.VMEM((TP, 5, F), f32),
        pltpu.VMEM((TP, Z, 4, F), bf),
        pltpu.VMEM((64, D), f32),
        pltpu.VMEM((Y, 64, 256), bf),
        pltpu.VMEM((2, TOK, D), bf),
        pltpu.VMEM((3, TOK, D), f32),
        pltpu.VMEM((128, D), bf),
        pltpu.VMEM((D, 128), bf),
        pltpu.VMEM((D, 256), bf),
        pltpu.VMEM((TP, 128, D), bf),
        pltpu.VMEM((TOK, D), bf),
        pltpu.VMEM((2, 14, COLS, 128), f32),
        pltpu.VMEM((3 * TOK, 128), bf),
        pltpu.VMEM((3 * TOK, 128), bf),
        pltpu.VMEM((ROWS, 128, 128), bf),
        pltpu.VMEM((ROWS, 128, 512), f32),
        pltpu.VMEM((TP, TOK, 128), bf),
        pltpu.VMEM((TOK, D), bf),
        dma((6,)),
        dma((TP,)),
    ]
    for n in (7, 7, 15, 15, 7, 7, 15, 15, 7, 7, 7, 7, 2, 2, 2, 2, 4, 4, 4, 4, 7, 7):
        scratch.append(dma((n,)))
    return pl.pallas_call(
        kernel,
        out_shape=jax.ShapeDtypeStruct((TOK, D), bf),
        in_specs=[any_, any_, vm, vm, vm, vm, vm, vm, any_, any_, any_, vm, vm, sm, any_],
        out_specs=any_,
        scratch_shapes=scratch,
        compiler_params=pltpu.CompilerParams(
            collective_id=0, has_side_effects=True, vmem_limit_bytes=56 * 1024 * 1024
        ),
        name="fused",
    )(
        latent, context, cond.reshape(1, 16), cctx.reshape(1, 16), shw, scw, gw, gain.reshape(1, D),
        wq, wk, wv, qg.reshape(1, HD), kg.reshape(1, HD), bias, outw,
    )


def solution(mesh):
    placed = (
        P("sp", None), P("sp", None), P("sp"), P("sp"),
        P("sp", "tp"), P("sp", "tp"), P("sp", "tp"), P(),
        P(None, "tp"), P(None, "tp"), P(None, "tp"), P(), P(),
        P("tp", None, None), P("tp", None),
    )
    return jax.shard_map(
        per_device, mesh=mesh, in_specs=placed, out_specs=P("sp", None), check_vma=False
    )
```

time: 237 us -> 77.6 us (0.33)
  blocking collectives: 115 us -> 0 us
  Pallas kernels: 0 us -> 73.7 us
  waiting for transfers between devices: 63.9 us -> 0 us
  other arithmetic: 15.9 us -> 0 us
  between operations: 13.8 us -> 0.01 us
  matrix products: 11.9 us -> 0 us
  local copies, waits for them, and re-layouts: 10.3 us -> 3.63 us
  starting transfers between devices: 5.94 us -> 0 us
    pallas_call x0 -> x1, Pallas kernels: none -> 73.7 us  [per_device(): pl.pallas_call(kernel, out_shape=jax.ShapeDtypeStruct((TOK, D), bf), in_s...]
    all_gather x1 -> x0, waiting for transfers between devices: 63.8 us -> none  [total_of_pieces(): tiles = lax.all_gather(x, axis).astype(jnp.float32)]
    all_gather x3 -> x0, blocking collectives: 63.1 us -> none  [the longest x2 38.6 us: all_blocks(): tiles = lax.all_gather(tiles, axes[k], axis=0, tiled=True)]
    psum x2 -> x0, blocking collectives: 51.6 us -> none  [by_axis(): x = lax.psum(x, axis)]
    dot_general x15 -> x0, matrix products: 11.9 us -> none  [the longest x1 2.41 us: per_device(): jnp.einsum('rja,haqk->hrqjk', row_hot, jnp.where(col_open[None, None], co...]
    reduce_sum x6 -> x0, other arithmetic: 7.72 us -> none  [the longest x1 5.48 us: total_of_pieces(): return tiles.sum(axis=0)]
    ppermute x2 -> x0, starting transfers between devices: 5.94 us -> none  [the longest x1 4.65 us: extended(): before = lax.ppermute(last, axis, up)]
    reshape x7 -> x0, local copies, waits for them, and re-layouts: 4.4 us -> none  [the longest x1 2.1 us: per_device(): offset_terms.reshape(heads_dev, local_rows, GRID_W, window_keys)]
  transfers between devices with their start and end apart: 3 -> 0, of which waited for: 1 -> 0; matrix products, arithmetic and copies ran while one was open for 4% -> 0% of each run, Pallas kernels for 0% -> 0%
where the time goes in v1:
time: 77.6 us; the launch traced here: 77.3 us
  Pallas kernels  73.7 us (95%)
  local copies, waits for them, and re-layouts  3.63 us (5%)
    pallas_call x1, Pallas kernels, per_device(): pl.pallas_call(kernel, out_shape=jax.ShapeDtypeStruct((TOK, D), bf), in_s...  73.7 us
    unnamed x2, local copies, waits for them, and re-layouts  3.63 us

profile of v1, /device:TPU:1, one launch (start us, length us, event | category | flops | bytes accessed | tf_op | source)
XLA Modules:
  0.0 77.3 jit_solution(13593735197110897081)
XLA Ops:
  0.0 1.3 %copy.16.bias = f32[2,15,31]{2,1,0:T(8,128)} copy(f32[2,15,31]{2,0,1:T(2,128)} %param.28) | data formatting | bytes 7440 | tf_op args[13]
  1.3 73.7 %fused.1 = bf16[256,2048]{1,0:T(8,128)(2,1)} custom-call(bf16[256,2048]{1,0:T(8,128)(2,1)} %latent.1, bf16[4,2048]{1,0:T(4,128)(2,1)} %context.1, f32[1,16]{1,0:T(1,128)} %bitcast.6, f32[1,16]{1,0:T(1,128)} %bitcast.7, bf16[16,256]{1,0:T(8,128)(2,1)} %shw.1, bf16[16,256]{1,0:T(8,128)(2,1)} %scw.1, bf16[16,256]{1,0:T(8,128)(2,1)} %gw.1, f32[1,2048]{1,0:T(1,128)} %bitcast.5, ...), custom_call_target="tpu_custom_call" | custom-call | tf_op jit(solution)/shard_map/fused/pallas_call | solution.py:375
  75.0 2.3 %copy.18 = bf16[256,2048]{1,0:T(8,128)(2,1)} copy(bf16[256,2048]{1,0:T(8,128)(2,1)} %fused.1) | data formatting | bytes 2097152

commit v2 on v1

v2 whole, which is shorter than its diff:
```python
import jax
import jax.numpy as jnp
from jax import lax
from jax.experimental import pallas as pl
from jax.experimental.pallas import tpu as pltpu
from jax.sharding import PartitionSpec as P

MESH = pl.DeviceIdType.MESH
EPS = 1e-06
Z, Y, TP = 16, 8, 8
SP = Z * Y
D = 2048
F = D // TP
TOK = 256
COLS = 64
ROWS = 4
HD = 64
HALF = D // 2
NEG = float("-inf")


def rem(a, n):
    return lax.rem(a, jnp.int32(n))


def head_norm(p, gain2):
    lane = lax.broadcasted_iota(jnp.int32, p.shape, 1)
    left = lane < HD
    sq = p * p
    s0 = jnp.sum(jnp.where(left, sq, 0.0), axis=1, keepdims=True)
    s1 = jnp.sum(jnp.where(left, 0.0, sq), axis=1, keepdims=True)
    r0 = lax.rsqrt(s0 * (1.0 / HD) + EPS)
    r1 = lax.rsqrt(s1 * (1.0 / HD) + EPS)
    return p * jnp.where(left, r0, r1) * gain2


def kernel(
    latent, context, cond_h, cctx_h, shw_h, scw_h, gw_h, gain_h, wq, wk, wv, qg_h, kg_h, bias_h, outw,
    out,
    cond, cctx, shw, scw, gw, gain, qg, kg, bias,
    part, mody, zpart, modz, modf,
    cbuf, cf, ckv,
    xn, hid, chid,
    wqv, wkvv, wfull, latv,
    tbl, kvp, q2, ec, attb, orem,
    small_sem, loc_sem,
    ys, yr, zs, zr, ts, tr,
    czs, czr, cts, ctr, cps, cpr, cys, cyr,
    hs, hr, ws, wr, fs, fr,
    as_, ar, aps, apr, os_, or_,
):
    sp = lax.axis_index("sp")
    tp = lax.axis_index("tp")
    y = rem(sp, Y)
    z = lax.div(sp, jnp.int32(Y))
    c = rem(tp, 2)
    mate = y + 1 - 2 * rem(y, 2)
    side = 2 * rem(y, 2) - 1
    pair = lax.div(y, jnp.int32(2))
    partner = tp + 1 - 2 * c
    up = rem(sp + 1, SP)
    down = rem(sp + SP - 1, SP)
    right = rem(tp + 2, TP)
    left = rem(tp + TP - 2, TP)
    far = rem(tp + 4, TP)

    def at(s, t):
        return {"sp": s, "tp": t}

    def y_peer(k):
        return at(z * Y + rem(y + k, Y), tp)

    def z_peer(k):
        return at(rem(z + k, Z) * Y + y, tp)

    def m_peer(k):
        return at(rem(z + k, Z) * Y + mate, tp)

    def t_peer(k):
        return at(sp, rem(tp + k, TP))

    def remote(src, dst, s, r, dev):
        return pltpu.make_async_remote_copy(
            src_ref=src, dst_ref=dst, send_sem=s, recv_sem=r, device_id=dev, device_id_type=MESH
        )

    sends = []

    def send(src, dst, s, r, dev):
        d = remote(src, dst, s, r, dev)
        d.start()
        sends.append(d)
        return d

    small = [
        pltpu.make_async_copy(src, dst, small_sem.at[n])
        for n, (src, dst) in enumerate(
            (
                (cond_h, cond), (cctx_h, cctx), (shw_h, shw), (scw_h, scw), (gw_h, gw),
                (bias_h, bias), (gain_h, gain), (qg_h, qg), (kg_h, kg),
            )
        )
    ]
    for d in small:
        d.start()
    ctx_col = pl.multiple_of(tp * F, F)
    my_half = pl.ds(pl.multiple_of(c * HALF, HALF), HALF)
    its_half = pl.ds(pl.multiple_of((1 - c) * HALF, HALF), HALF)
    own_ctx = cbuf.at[tp, y - 2 * pair, z]
    own_c = pltpu.make_async_copy(context.at[:, pl.ds(ctx_col, F)], own_ctx, loc_sem.at[0])
    own_l = pltpu.make_async_copy(latent, latv, loc_sem.at[1])
    own_q = pltpu.make_async_copy(wq, wqv, loc_sem.at[2])
    own_k = pltpu.make_async_copy(wk, wkvv.at[:, pl.ds(0, 128)], loc_sem.at[3])
    own_v = pltpu.make_async_copy(wv, wkvv.at[:, pl.ds(128, 128)], loc_sem.at[4])
    own_w = pltpu.make_async_copy(outw.at[:, my_half], wfull.at[tp], loc_sem.at[5])
    own_c.start()
    own_l.start()
    own_q.start()
    own_k.start()
    own_v.start()
    own_w.start()

    barrier = pltpu.get_barrier_semaphore()
    z_order = (8, 7, 9, 6, 10, 5, 11, 4, 12, 3, 13, 2, 14, 1, 15)
    y_order = (4, 3, 5, 2, 6, 1, 7)
    peers = [z_peer(k) for k in z_order] + [m_peer(k) for k in z_order + (0,)]
    peers += [y_peer(k) for k in y_order]
    peers += [t_peer(k) for k in range(1, TP)]
    peers += [at(up, tp), at(down, tp)]
    for p in peers:
        pl.semaphore_signal(barrier, inc=1, device_id=p, device_id_type=MESH)

    for d in small:
        d.wait()
    row8 = lax.broadcasted_iota(jnp.int32, (8, 16), 0)
    pre = jnp.where(row8 == 0, jnp.broadcast_to(cond[...], (8, 16)), jnp.broadcast_to(cctx[...], (8, 16)))
    act = (pre / (1.0 + jnp.exp(-pre))).astype(jnp.bfloat16)
    p_sh = jnp.dot(act, shw[...], preferred_element_type=jnp.float32)
    p_sc = jnp.dot(act, scw[...], preferred_element_type=jnp.float32)
    p_g = jnp.dot(act, gw[...], preferred_element_type=jnp.float32)
    part[0:2, :] = p_sh[0:2]
    part[2:4, :] = p_sc[0:2]
    part[4:5, :] = p_g[0:1]
    own_c.wait()

    pl.semaphore_wait(barrier, len(peers))

    for k in y_order:
        send(part, mody.at[k - 1], ys.at[k - 1], yr.at[k - 1], y_peer(k))
    for k in z_order:
        send(own_ctx, own_ctx, czs.at[k], czr.at[k], z_peer(k))
        send(own_ctx, own_ctx, czs.at[Z + k], czr.at[Z + k], m_peer(k))
    send(own_ctx, own_ctx, czs.at[Z], czr.at[Z], m_peer(0))
    send(outw.at[:, its_half], wfull.at[tp], ws.at[0], wr.at[0], at(sp, partner))
    send(outw.at[:, my_half], wfull.at[tp], ws.at[1], wr.at[1], at(sp, right))
    send(outw.at[:, my_half], wfull.at[tp], ws.at[2], wr.at[2], at(sp, left))

    tq = lax.broadcasted_iota(jnp.int32, (COLS, 128), 0)
    tl = lax.broadcasted_iota(jnp.int32, (COLS, 128), 1)
    tk = jnp.where(tl < COLS, tl, tl - COLS)
    diff = tk - tq + 15
    c0 = jnp.clip(tq - 8, 0, 48)
    is_open = (tk >= c0) & (tk < c0 + 16)
    first = lax.broadcasted_iota(jnp.int32, (1, 128), 1) < COLS

    def table_step(n, carry):
        h = lax.div(n, jnp.int32(14))
        a = rem(n, 14)
        val = jnp.full((COLS, 128), NEG, jnp.float32)
        for dd in range(31):
            v = jnp.where(first, bias[a, h, dd], bias[a + 1, h, dd])
            val = jnp.where(diff == dd, jnp.broadcast_to(v, (COLS, 128)), val)
        tbl[h, a] = jnp.where(is_open, val, NEG)
        return carry

    lax.fori_loop(0, 28, table_step, 0)

    def normed(load, store, rows, chunk):
        def step(n, carry):
            r = pl.ds(pl.multiple_of(n * chunk, chunk), chunk)
            v = load(r).astype(jnp.float32)
            ms = jnp.mean(v * v, axis=-1, keepdims=True)
            store(r, v * lax.rsqrt(ms + EPS) * gain[...])
            return carry

        lax.fori_loop(0, rows // chunk, step, 0)

    acc = part[...]
    for k in range(1, Y):
        remote(part, mody.at[k - 1], ys.at[k - 1], yr.at[k - 1], y_peer(k)).wait_recv()
        acc = acc + mody[k - 1]
    zpart[...] = acc
    for k in z_order:
        send(zpart, modz.at[k - 1], zs.at[k - 1], zr.at[k - 1], z_peer(k))

    own_l.wait()

    def store_own(r, v):
        xn[r, :] = v

    normed(lambda r: latv[r, :], store_own, TOK, 16)

    for k in z_order:
        remote(own_ctx, own_ctx, czs.at[k], czr.at[k], z_peer(k)).wait_recv()
    for k in z_order + (0,):
        remote(own_ctx, own_ctx, czs.at[Z + k], czr.at[Z + k], m_peer(k)).wait_recv()
    hops = ((far, 0), (right, 1), (left, 2), (partner, 3))
    for t, n in hops:
        send(cbuf.at[tp], cbuf.at[tp], cts.at[n], ctr.at[n], at(sp, t))

    acc = zpart[...]
    for k in range(1, Z):
        remote(zpart, modz.at[k - 1], zs.at[k - 1], zr.at[k - 1], z_peer(k)).wait_recv()
        acc = acc + modz[k - 1]
    modf[tp] = acc
    for k in (4, 3, 5, 2, 6, 1, 7):
        send(modf.at[tp], modf.at[tp], ts.at[k - 1], tr.at[k - 1], t_peer(k))

    for t, n, frm in ((right, 1, left), (left, 2, right), (far, 0, far)):
        remote(cbuf.at[tp], cbuf.at[tp], cts.at[n], ctr.at[n], at(sp, t)).wait_recv()
        send(cbuf.at[frm], cbuf.at[frm], cps.at[n], cpr.at[n], at(sp, partner))
    remote(cbuf.at[tp], cbuf.at[tp], cts.at[3], ctr.at[3], at(sp, partner)).wait_recv()
    for n in range(3):
        remote(cbuf.at[tp], cbuf.at[tp], cps.at[n], cpr.at[n], at(sp, partner)).wait_recv()

    for j in range(2 * Z):
        for g in range(TP):
            cf[4 * j : 4 * j + 4, g * F : (g + 1) * F] = cbuf[g, j % 2, j // 2].astype(jnp.float32)

    def store_ctx(r, v):
        cf[r, :] = v

    normed(lambda r: cf[r, :], store_ctx, 128, 16)

    for k in range(1, TP):
        remote(modf.at[tp], modf.at[tp], ts.at[k - 1], tr.at[k - 1], t_peer(k)).wait_recv()

    own_k.wait()
    own_v.wait()
    own_q.wait()
    lane = lax.broadcasted_iota(jnp.int32, (1, 128), 1)
    qg2 = jnp.concatenate([qg[...], qg[...]], axis=1)
    kg2 = jnp.concatenate([kg[...], kg[...]], axis=1)

    for g in range(TP):
        gs = slice(g * F, (g + 1) * F)
        chid[:, gs] = (cf[:, gs] * (1.0 + modf[g, 3:4, :]) + modf[g, 1:2, :]).astype(jnp.bfloat16)
    kv = jnp.dot(chid[...], wkvv[...], preferred_element_type=jnp.float32)
    ckv[pair, :, 0:128] = head_norm(kv[:, 0:128], kg2).astype(jnp.bfloat16)
    ckv[pair, :, 128:256] = kv[:, 128:256].astype(jnp.bfloat16)
    own_pair = ckv.at[pair]
    for k in (3, 2, 1):
        send(own_pair, own_pair, cys.at[k - 1], cyr.at[k - 1], at(z * Y + rem(y + side * k + Y, Y), tp))

    lo, hi = pl.ds(0, 64), pl.ds(64, 64)

    def w_wait(n, t):
        remote(wfull.at[tp], wfull.at[tp], ws.at[n], wr.at[n], at(sp, t)).wait_recv()

    def w_forward(n, frm_left, frm_right):
        send(wfull.at[frm_left, lo], wfull.at[frm_left, lo], fs.at[n], fr.at[n], at(sp, right))
        send(wfull.at[frm_right, hi], wfull.at[frm_right, hi], fs.at[n + 1], fr.at[n + 1], at(sp, left))

    def other(t):
        return t + 1 - 2 * c

    send(outw.at[:, its_half], wfull.at[tp], ws.at[3], wr.at[3], at(sp, other(right)))
    send(outw.at[:, its_half], wfull.at[tp], ws.at[4], wr.at[4], at(sp, other(left)))
    w_wait(1, right)
    w_wait(2, left)
    w_forward(0, left, right)

    for n in range(2):
        r = pl.ds(n * 128, 128)
        for g in range(TP):
            gs = slice(g * F, (g + 1) * F)
            hid[r, gs] = (xn[r, gs] * (1.0 + modf[g, 2:3, :]) + modf[g, 0:1, :]).astype(jnp.bfloat16)
        h = hid[r, :]
        kv = jnp.dot(h, wkvv[...], preferred_element_type=jnp.float32)
        kr = pl.ds(TOK + n * 128, 128)
        kvp[kr, 0:128] = head_norm(kv[:, 0:128], kg2).astype(jnp.bfloat16)
        kvp[kr, 128:256] = kv[:, 128:256].astype(jnp.bfloat16)
    own_rows = kvp.at[pl.ds(TOK, TOK)]
    send(own_rows, kvp.at[pl.ds(0, TOK)], hs.at[0], hr.at[0], at(up, tp))
    send(own_rows, kvp.at[pl.ds(2 * TOK, TOK)], hs.at[1], hr.at[1], at(down, tp))
    for n in range(2):
        r = pl.ds(n * 128, 128)
        q = jnp.dot(hid[r, :], wqv[...], preferred_element_type=jnp.float32)
        q = (head_norm(q, qg2) * (HD**-0.5)).astype(jnp.bfloat16)
        zero = jnp.zeros_like(q)
        lf = jnp.broadcast_to(lane < HD, q.shape)
        q0 = jnp.where(lf, q, zero)
        q1 = jnp.where(lf, zero, q)
        for i in range(2):
            q2[2 * n + i, 0:64, :] = q0[i * 64 : (i + 1) * 64]
            q2[2 * n + i, 64:128, :] = q1[i * 64 : (i + 1) * 64]

    w_wait(3, other(right))
    w_wait(4, other(left))
    w_forward(2, other(left), other(right))

    nt = (((1,), (1,)), ((), ()))
    for k in (1, 2, 3):
        remote(own_pair, own_pair, cys.at[k - 1], cyr.at[k - 1], at(z * Y + mate, tp)).wait_recv()
    ck = ckv[:, :, 0:128].reshape(512, 128)
    m_c, l_c = [], []
    for i in range(ROWS):
        s = lax.dot_general(q2[i], ck, nt, preferred_element_type=jnp.float32)
        m = jnp.max(s, axis=1, keepdims=True)
        e = jnp.exp(s - m)
        ec[i] = e
        m_c.append(m)
        l_c.append(jnp.sum(e, axis=1, keepdims=True))

    for n in range(2):
        remote(own_rows, kvp.at[pl.ds(0, TOK)], hs.at[n], hr.at[n], at(up, tp)).wait_recv()

    at_first = sp == 0
    at_last = sp == SP - 1
    cv = ckv[:, :, 128:256].reshape(512, 128)
    for i in range(ROWS):
        start = jnp.where(at_first, 4, jnp.where(at_last, 0, i))
        off = jnp.where(at_first, 7 - i, 3 + jnp.where(at_last, -i, 0))
        rows = pl.ds(pl.multiple_of(start * COLS, COLS), 8 * COLS)
        s = lax.dot_general(q2[i], kvp[rows, 0:128], nt, preferred_element_type=jnp.float32)
        tiles = []
        for p in range(4):
            t = jnp.concatenate([tbl[0, off + 2 * p], tbl[1, off + 2 * p]], axis=0)
            tiles.append(s[:, p * 128 : (p + 1) * 128] + t)
        s = jnp.concatenate(tiles, axis=1)
        m = jnp.maximum(m_c[i], jnp.max(s, axis=1, keepdims=True))
        ew = jnp.exp(s - m)
        fc = jnp.exp(m_c[i] - m)
        inv = 1.0 / (l_c[i] * fc + jnp.sum(ew, axis=1, keepdims=True))
        w_win = (ew * inv).astype(jnp.bfloat16)
        w_ctx = (ec[i] * (fc * inv)).astype(jnp.bfloat16)
        o = jnp.dot(w_win, kvp[rows, 128:256], preferred_element_type=jnp.float32) + jnp.dot(
            w_ctx, cv, preferred_element_type=jnp.float32
        )
        o = jnp.where(jnp.broadcast_to(lane < HD, (64, 128)), o[0:64], o[64:128])
        attb[tp, i * COLS : (i + 1) * COLS, :] = o.astype(jnp.bfloat16)
        if i % 2 == 1:
            hh = i // 2
            block = attb.at[tp, pl.ds(hh * 128, 128)]
            for t, n in hops:
                send(block, block, as_.at[hh * 4 + n], ar.at[hh * 4 + n], at(sp, t))

    for hh in range(2):
        rr = pl.ds(hh * 128, 128)
        block = attb.at[tp, rr]
        for t, n, frm in ((right, 1, left), (left, 2, right), (far, 0, far)):
            remote(block, block, as_.at[hh * 4 + n], ar.at[hh * 4 + n], at(sp, t)).wait_recv()
            b = attb.at[frm, rr]
            send(b, b, aps.at[hh * 3 + n], apr.at[hh * 3 + n], at(sp, partner))

    w_wait(0, partner)
    own_w.wait()
    for n in range(4):
        remote(wfull.at[left, lo], wfull.at[far, lo], fs.at[n], fr.at[n], at(sp, right)).wait_recv()

    for hh in range(2):
        rr = pl.ds(hh * 128, 128)
        block = attb.at[tp, rr]
        remote(block, block, as_.at[hh * 4 + 3], ar.at[hh * 4 + 3], at(sp, partner)).wait_recv()
        for n in range(3):
            remote(block, block, aps.at[hh * 3 + n], apr.at[hh * 3 + n], at(sp, partner)).wait_recv()
        for n in range(HALF // F):
            cols = pl.ds(pl.multiple_of(c * HALF + n * F, F), F)
            acc = jnp.zeros((128, F), jnp.float32)
            for g in range(TP):
                t = jnp.dot(attb[g, rr, :], wfull[g, :, n * F : (n + 1) * F], preferred_element_type=jnp.float32)
                acc = acc + t.astype(jnp.bfloat16).astype(jnp.float32)
            res = latv[rr, cols].astype(jnp.float32) + modf[c * (HALF // F) + n, 4:5, :] * acc
            out[rr, cols] = res.astype(jnp.bfloat16)
        send(out.at[rr, my_half], orem.at[rr], os_.at[hh], or_.at[hh], at(sp, partner))
    for hh in range(2):
        rr = pl.ds(hh * 128, 128)
        remote(orem.at[rr], orem.at[rr], os_.at[hh], or_.at[hh], at(sp, partner)).wait_recv()
        out[rr, its_half] = orem[rr, :]

    for d in sends:
        d.wait_send()


def per_device(latent, context, cond, cctx, shw, scw, gw, gain, wq, wk, wv, qg, kg, bias, outw):
    hbm = pl.BlockSpec(memory_space=pltpu.HBM)
    vm = pl.BlockSpec(memory_space=pltpu.VMEM)
    bf, f32 = jnp.bfloat16, jnp.float32
    dma = pltpu.SemaphoreType.DMA
    scratch = [
        pltpu.VMEM((1, 16), f32),
        pltpu.VMEM((1, 16), f32),
        pltpu.VMEM((16, F), bf),
        pltpu.VMEM((16, F), bf),
        pltpu.VMEM((16, F), bf),
        pltpu.VMEM((1, D), f32),
        pltpu.VMEM((1, HD), f32),
        pltpu.VMEM((1, HD), f32),
        pltpu.SMEM((15, 2, 31), f32),
        pltpu.VMEM((5, F), f32),
        pltpu.VMEM((Y - 1, 5, F), f32),
        pltpu.VMEM((5, F), f32),
        pltpu.VMEM((Z - 1, 5, F), f32),
        pltpu.VMEM((TP, 5, F), f32),
        pltpu.VMEM((TP, 2, Z, 4, F), bf),
        pltpu.VMEM((128, D), f32),
        pltpu.VMEM((4, 128, 256), bf),
        pltpu.VMEM((TOK, D), f32),
        pltpu.VMEM((TOK, D), bf),
        pltpu.VMEM((128, D), bf),
        pltpu.VMEM((D, 128), bf),
        pltpu.VMEM((D, 256), bf),
        pltpu.VMEM((TP, 128, HALF), bf),
        pltpu.VMEM((TOK, D), bf),
        pltpu.VMEM((2, 14, COLS, 128), f32),
        pltpu.VMEM((3 * TOK, 256), bf),
        pltpu.VMEM((ROWS, 128, 128), bf),
        pltpu.VMEM((ROWS, 128, 512), f32),
        pltpu.VMEM((TP, TOK, 128), bf),
        pltpu.VMEM((TOK, HALF), bf),
        dma((9,)),
        dma((6,)),
    ]
    for n in (7, 15, 7, 32, 4, 3, 3, 2, 5, 4, 8, 6, 2):
        scratch += [dma((n,)), dma((n,))]
    return pl.pallas_call(
        kernel,
        out_shape=jax.ShapeDtypeStruct((TOK, D), bf),
        in_specs=[hbm] * 15,
        out_specs=vm,
        scratch_shapes=scratch,
        compiler_params=pltpu.CompilerParams(
            collective_id=0, has_side_effects=True, vmem_limit_bytes=40 * 1024 * 1024
        ),
        name="fused",
    )(
        *(
            pltpu.with_memory_space_constraint(a, pltpu.HBM)
            for a in (
                latent, context, cond.reshape(1, 16), cctx.reshape(1, 16), shw, scw, gw, gain.reshape(1, D),
                wq, wk, wv, qg.reshape(1, HD), kg.reshape(1, HD), bias.transpose(1, 0, 2), outw,
            )
        )
    )


def solution(mesh):
    placed = (
        P("sp", None), P("sp", None), P("sp"), P("sp"),
        P("sp", "tp"), P("sp", "tp"), P("sp", "tp"), P(),
        P(None, "tp"), P(None, "tp"), P(None, "tp"), P(), P(),
        P("tp", None, None), P("tp", None),
    )
    return jax.shard_map(
        per_device, mesh=mesh, in_specs=placed, out_specs=P("sp", None), check_vma=False
    )
```

time: 77.6 us -> 65.1 us (0.84)
  Pallas kernels: 73.7 us -> 63.9 us
  local copies, waits for them, and re-layouts: 3.63 us -> 0.97 us
    pallas_call x1, Pallas kernels: 73.7 us -> 63.9 us  [per_device(): pl.pallas_call(kernel, out_shape=jax.ShapeDtypeStruct((TOK, D), bf), in_s...]
    unnamed x2 -> x1, local copies, waits for them, and re-layouts: 3.63 us -> 0.97 us
where the time goes in v2:
time: 65.1 us; the launch traced here: 64.9 us
  Pallas kernels  63.9 us (98%)
  local copies, waits for them, and re-layouts  0.97 us (1%)
    pallas_call x1, Pallas kernels, per_device(): pl.pallas_call(kernel, out_shape=jax.ShapeDtypeStruct((TOK, D), bf), in_s...  63.9 us

profile of v2, /device:TPU:1, one launch (start us, length us, event | category | flops | bytes accessed | tf_op | source)
XLA Modules:
  0.0 64.9 jit_solution(14544035660403809320)
XLA Ops:
  0.0 63.9 %fused.1 = bf16[256,2048]{1,0:T(8,128)(2,1)S(1)} custom-call(bf16[256,2048]{1,0:T(8,128)(2,1)} %latent.1, bf16[4,2048]{1,0:T(4,128)(2,1)} %context.1, f32[1,16]{1,0:T(1,128)} %bitcast.8, f32[1,16]{1,0:T(1,128)} %bitcast.9, bf16[16,256]{1,0:T(8,128)(2,1)} %shw_h.1, bf16[16,256]{1,0:T(8,128)(2,1)} %scw_h.1, bf16[16,256]{1,0:T(8,128)(2,1)} %gw_h.1, ...), custom_call_target="tpu_custom_call" | custom-call | tf_op jit(solution)/shard_map/fused/pallas_call | solution.py:426
  63.9 1.0 %copy.17 = bf16[256,2048]{1,0:T(8,128)(2,1)} copy(bf16[256,2048]{1,0:T(8,128)(2,1)S(1)} %fused.1) | data formatting | bytes 2097152

commit v3 on v2

v3 whole, which is shorter than its diff:
```python
import jax
import jax.numpy as jnp
from jax import lax
from jax.experimental import pallas as pl
from jax.experimental.pallas import tpu as pltpu
from jax.sharding import PartitionSpec as P

MESH = pl.DeviceIdType.MESH
EPS = 1e-06
Z, Y, TP = 16, 8, 8
SP = Z * Y
D = 2048
F = D // TP
TOK = 256
COLS = 64
ROWS = 4
HD = 64
HALF = D // 2
NEG = float("-inf")


def rem(a, n):
    return lax.rem(a, jnp.int32(n))


def head_norm(p, gain2):
    lane = lax.broadcasted_iota(jnp.int32, p.shape, 1)
    left = lane < HD
    sq = p * p
    s0 = jnp.sum(jnp.where(left, sq, 0.0), axis=1, keepdims=True)
    s1 = jnp.sum(jnp.where(left, 0.0, sq), axis=1, keepdims=True)
    r0 = lax.rsqrt(s0 * (1.0 / HD) + EPS)
    r1 = lax.rsqrt(s1 * (1.0 / HD) + EPS)
    return p * jnp.where(left, r0, r1) * gain2


def kernel(
    latent, context, cond_h, cctx_h, shw_h, scw_h, gw_h, gain_h, wq, wk, wv, qg_h, kg_h, bias_h, outw,
    out,
    cc, modw, gain, qkg, bias,
    part, mody, zpart, modz, modf,
    cbuf, cf, ckv,
    xn, hid, chid,
    wall, wfull, latv,
    tbl, kvp, q2, ew, attb,
    relay, small_sem, loc_sem,
    ys, yr, zs, zr, ts, tr,
    czs, czr, cts, ctr, cpr, cys, cyr,
    hs, hr, ws, wr,
    as_, ar, apr, os_, or_,
):
    sp = lax.axis_index("sp")
    tp = lax.axis_index("tp")
    y = rem(sp, Y)
    z = lax.div(sp, jnp.int32(Y))
    c = rem(tp, 2)
    odd = rem(y, 2)
    mate = y + 1 - 2 * odd
    side = 2 * odd - 1
    pair = lax.div(y, jnp.int32(2))
    partner = tp + 1 - 2 * c
    up = rem(sp + 1, SP)
    down = rem(sp + SP - 1, SP)
    right = rem(tp + 2, TP)
    left = rem(tp + TP - 2, TP)
    far = rem(tp + 4, TP)

    def at(s, t):
        return {"sp": s, "tp": t}

    def y_peer(k):
        return at(z * Y + rem(y + k, Y), tp)

    def z_peer(k):
        return at(rem(z + k, Z) * Y + y, tp)

    def m_peer(k):
        return at(rem(z + k, Z) * Y + mate, tp)

    def t_peer(k):
        return at(sp, rem(tp + k, TP))

    def remote(src, dst, s, r, dev):
        return pltpu.make_async_remote_copy(
            src_ref=src, dst_ref=dst, send_sem=s, recv_sem=r, device_id=dev, device_id_type=MESH
        )

    def send(src, dst, s, r, dev):
        remote(src, dst, s, r, dev).start()

    def arrived(ref, r):
        remote(ref, ref, r, r, at(sp, partner)).wait_recv()

    def sent(ref, s):
        remote(ref, ref, s, s, at(sp, partner)).wait_send()

    barrier = pltpu.get_barrier_semaphore()
    near = (4, 12, 3, 13, 2, 14, 1, 15)
    beyond = (8, 7, 9, 6, 10, 5, 11)
    y_order = (4, 3, 5, 2, 6, 1, 7)
    peers = [y_peer(k) for k in y_order]
    peers += [z_peer(k) for k in near] + [m_peer(k) for k in near + (0,)]
    peers += [t_peer(k) for k in range(1, TP)]
    peers += [at(up, tp), at(down, tp)]
    for p in peers:
        pl.semaphore_signal(barrier, inc=1, device_id=p, device_id_type=MESH)

    small = (
        (cond_h, cc.at[0], 0), (cctx_h, cc.at[1], 0),
        (shw_h, modw.at[0], 1), (scw_h, modw.at[1], 1), (gw_h, modw.at[2], 1),
        (bias_h, bias, 2), (gain_h, gain, 3), (qg_h, qkg.at[0], 4), (kg_h, qkg.at[1], 4),
    )
    for src, dst, n in small:
        pltpu.make_async_copy(src, dst, small_sem.at[n]).start()
    ctx_col = pl.multiple_of(tp * F, F)
    my_half = pl.ds(pl.multiple_of(c * HALF, HALF), HALF)
    its_half = pl.ds(pl.multiple_of((1 - c) * HALF, HALF), HALF)
    own_ctx = cbuf.at[tp, odd, z]
    own_c = pltpu.make_async_copy(context.at[:, pl.ds(ctx_col, F)], own_ctx, loc_sem.at[0])
    own_l = pltpu.make_async_copy(latent, latv, loc_sem.at[1])
    own_w = pltpu.make_async_copy(outw.at[:, my_half], wfull.at[tp], loc_sem.at[2])
    own_c.start()
    own_l.start()
    own_w.start()
    for n, src in enumerate((wk, wv, wq)):
        pltpu.make_async_copy(src, wall.at[:, pl.ds(n * 128, 128)], loc_sem.at[3]).start()

    pl.semaphore_wait(barrier, len(peers))
    for k in (4, Z - 4):
        pl.semaphore_signal(relay, inc=1, device_id=z_peer(k), device_id_type=MESH)

    pltpu.make_async_copy(cc, cc, small_sem.at[0]).wait()
    pltpu.make_async_copy(modw, modw, small_sem.at[1]).wait()
    row8 = lax.broadcasted_iota(jnp.int32, (8, 16), 0)
    pre = jnp.where(row8 == 0, jnp.broadcast_to(cc[0], (8, 16)), jnp.broadcast_to(cc[1], (8, 16)))
    act = (pre / (1.0 + jnp.exp(-pre))).astype(jnp.bfloat16)
    p_sh = jnp.dot(act, modw[0], preferred_element_type=jnp.float32)
    p_sc = jnp.dot(act, modw[1], preferred_element_type=jnp.float32)
    p_g = jnp.dot(act, modw[2], preferred_element_type=jnp.float32)
    part[0:2, :] = p_sh[0:2]
    part[2:4, :] = p_sc[0:2]
    part[4:5, :] = p_g[0:1]

    def other(t):
        return t + 1 - 2 * c

    for k in y_order:
        send(part, mody.at[k - 1], ys, yr, y_peer(k))
    own_c.wait()
    for k in near:
        send(own_ctx, own_ctx, czs.at[0], czr.at[0], z_peer(k))
        send(own_ctx, own_ctx, czs.at[1], czr.at[1], m_peer(k))
    send(own_ctx, own_ctx, czs.at[1], czr.at[1], m_peer(0))
    send(outw.at[:, its_half], wfull.at[tp], ws, wr.at[0], at(sp, partner))
    send(outw.at[:, my_half], wfull.at[tp], ws, wr.at[1], at(sp, right))
    send(outw.at[:, my_half], wfull.at[tp], ws, wr.at[1], at(sp, left))
    send(outw.at[:, its_half], wfull.at[tp], ws, wr.at[2], at(sp, other(right)))
    send(outw.at[:, its_half], wfull.at[tp], ws, wr.at[2], at(sp, other(left)))

    pl.semaphore_wait(relay, 2)
    for k in beyond:
        send(own_ctx, own_ctx, czs.at[0], czr.at[0], z_peer(k))
        send(own_ctx, own_ctx, czs.at[1], czr.at[1], m_peer(k))

    arrived(mody, yr)
    acc = part[...]
    for k in range(1, Y):
        acc = acc + mody[k - 1]
    zpart[...] = acc
    for k in beyond + near:
        send(zpart, modz.at[k - 1], zs, zr, z_peer(k))

    tq = lax.broadcasted_iota(jnp.int32, (COLS, 128), 0)
    tl = lax.broadcasted_iota(jnp.int32, (COLS, 128), 1)
    tk = jnp.where(tl < COLS, tl, tl - COLS)
    diff = tk - tq + 15
    c0 = jnp.clip(tq - 8, 0, 48)
    is_open = (tk >= c0) & (tk < c0 + 16)
    first = lax.broadcasted_iota(jnp.int32, (1, 128), 1) < COLS

    def table_step(n, carry):
        h = lax.div(n, jnp.int32(14))
        a = rem(n, 14)
        val = jnp.full((COLS, 128), NEG, jnp.float32)
        for dd in range(31):
            v = jnp.where(first, bias[a, h, dd], bias[a + 1, h, dd])
            val = jnp.where(diff == dd, jnp.broadcast_to(v, (COLS, 128)), val)
        tbl[h, a] = jnp.where(is_open, val, NEG)
        return carry

    pltpu.make_async_copy(bias_h, bias, small_sem.at[2]).wait()
    lax.fori_loop(0, 28, table_step, 0)
    pltpu.make_async_copy(gain_h, gain, small_sem.at[3]).wait()

    def normed(load, store, rows, chunk):
        def step(n, carry):
            r = pl.ds(pl.multiple_of(n * chunk, chunk), chunk)
            v = load(r).astype(jnp.float32)
            ms = jnp.mean(v * v, axis=-1, keepdims=True)
            store(r, v * lax.rsqrt(ms + EPS) * gain[...])
            return carry

        lax.fori_loop(0, rows // chunk, step, 0)

    own_l.wait()

    def store_own(r, v):
        xn[r, :] = v

    normed(lambda r: latv[r, :], store_own, TOK, 16)

    arrived(cbuf.at[0, 0, pl.ds(0, Z - 1)], czr.at[0])
    arrived(cbuf.at[0, 0], czr.at[1])
    hops = ((far, 0), (right, 1), (left, 2), (partner, 3))
    for t, n in hops:
        send(cbuf.at[tp], cbuf.at[tp], cts, ctr.at[n], at(sp, t))

    arrived(modz, zr)
    acc = zpart[...]
    for k in range(1, Z):
        acc = acc + modz[k - 1]
    modf[tp] = acc
    for k in (4, 3, 5, 2, 6, 1, 7):
        send(modf.at[tp], modf.at[tp], ts, tr, t_peer(k))

    for n, frm in ((1, left), (2, right), (0, far)):
        arrived(cbuf.at[frm], ctr.at[n])
        send(cbuf.at[frm], cbuf.at[frm], cts, cpr, at(sp, partner))

    pltpu.make_async_copy(wall, wall, loc_sem.at[3]).wait()
    pltpu.make_async_copy(qkg, qkg, small_sem.at[4]).wait()
    arrived(modf.at[pl.ds(0, TP - 1)], tr)
    lane = lax.broadcasted_iota(jnp.int32, (1, 128), 1)
    qg2 = jnp.concatenate([qkg[0], qkg[0]], axis=1)
    kg2 = jnp.concatenate([qkg[1], qkg[1]], axis=1)

    for n in range(2):
        r = pl.ds(n * 128, 128)
        for g in range(TP):
            gs = slice(g * F, (g + 1) * F)
            hid[r, gs] = (xn[r, gs] * (1.0 + modf[g, 2:3, :]) + modf[g, 0:1, :]).astype(jnp.bfloat16)
        h = hid[r, :]
        kv = jnp.dot(h, wall[:, 0:256], preferred_element_type=jnp.float32)
        kr = pl.ds(TOK + n * 128, 128)
        kvp[kr, 0:128] = head_norm(kv[:, 0:128], kg2).astype(jnp.bfloat16)
        kvp[kr, 128:256] = kv[:, 128:256].astype(jnp.bfloat16)
    own_rows = kvp.at[pl.ds(TOK, TOK)]
    send(own_rows, kvp.at[pl.ds(0, TOK)], hs, hr, at(up, tp))
    send(own_rows, kvp.at[pl.ds(2 * TOK, TOK)], hs, hr, at(down, tp))

    arrived(cbuf.at[partner], ctr.at[3])
    arrived(cbuf.at[pl.ds(0, 3)], cpr)

    for j in range(2 * Z):
        for g in range(TP):
            cf[4 * j : 4 * j + 4, g * F : (g + 1) * F] = cbuf[g, j % 2, j // 2].astype(jnp.float32)

    def store_ctx(r, v):
        cf[r, :] = v

    normed(lambda r: cf[r, :], store_ctx, 128, 16)

    for g in range(TP):
        gs = slice(g * F, (g + 1) * F)
        chid[:, gs] = (cf[:, gs] * (1.0 + modf[g, 3:4, :]) + modf[g, 1:2, :]).astype(jnp.bfloat16)
    kv = jnp.dot(chid[...], wall[:, 0:256], preferred_element_type=jnp.float32)
    ckv[pair, :, 0:128] = head_norm(kv[:, 0:128], kg2).astype(jnp.bfloat16)
    ckv[pair, :, 128:256] = kv[:, 128:256].astype(jnp.bfloat16)
    own_pair = ckv.at[pair]
    send(own_pair, own_pair, cys, cyr.at[0], at(z * Y + rem(y + side + Y, Y), tp))
    send(own_pair, own_pair, cys, cyr.at[1], at(z * Y + rem(y + 3 * side + Y, Y), tp))

    for n in range(2):
        r = pl.ds(n * 128, 128)
        q = jnp.dot(hid[r, :], wall[:, 256:384], preferred_element_type=jnp.float32)
        q = (head_norm(q, qg2) * (HD**-0.5)).astype(jnp.bfloat16)
        zero = jnp.zeros_like(q)
        lf = jnp.broadcast_to(lane < HD, q.shape)
        q0 = jnp.where(lf, q, zero)
        q1 = jnp.where(lf, zero, q)
        for i in range(2):
            q2[2 * n + i, 0:64, :] = q0[i * 64 : (i + 1) * 64]
            q2[2 * n + i, 64:128, :] = q1[i * 64 : (i + 1) * 64]

    lo, hi = pl.ds(0, 64), pl.ds(64, 64)
    arrived(wfull.at[pl.ds(0, 2)], wr.at[1])
    arrived(wfull.at[pl.ds(0, 2)], wr.at[2])
    for f in (left, other(left)):
        send(wfull.at[f, lo], wfull.at[f, lo], ws, wr.at[3], at(sp, right))
    for f in (right, other(right)):
        send(wfull.at[f, hi], wfull.at[f, hi], ws, wr.at[3], at(sp, left))

    near_pair = ckv.at[rem(pair + side + 4, 4)]
    arrived(near_pair, cyr.at[0])
    send(near_pair, near_pair, cys, cyr.at[1], at(z * Y + mate, tp))

    arrived(kvp.at[pl.ds(0, 2 * TOK)], hr)

    nt = (((1,), (1,)), ((), ()))
    at_first = sp == 0
    at_last = sp == SP - 1
    m_w, l_w, band = [], [], []
    for i in range(ROWS):
        start = jnp.where(at_first, 4, jnp.where(at_last, 0, i))
        off = jnp.where(at_first, 7 - i, 3 + jnp.where(at_last, -i, 0))
        rows = pl.ds(pl.multiple_of(start * COLS, COLS), 8 * COLS)
        band.append(rows)
        s = lax.dot_general(q2[i], kvp[rows, 0:128], nt, preferred_element_type=jnp.float32)
        tiles = []
        for p in range(4):
            t = jnp.concatenate([tbl[0, off + 2 * p], tbl[1, off + 2 * p]], axis=0)
            tiles.append(s[:, p * 128 : (p + 1) * 128] + t)
        s = jnp.concatenate(tiles, axis=1)
        m = jnp.max(s, axis=1, keepdims=True)
        e = jnp.exp(s - m)
        ew[i] = e
        m_w.append(m)
        l_w.append(jnp.sum(e, axis=1, keepdims=True))

    arrived(ckv.at[pl.ds(0, 2)], cyr.at[1])

    ck = ckv[:, :, 0:128].reshape(512, 128)
    cv = ckv[:, :, 128:256].reshape(512, 128)
    for i in range(ROWS):
        s = lax.dot_general(q2[i], ck, nt, preferred_element_type=jnp.float32)
        m = jnp.maximum(m_w[i], jnp.max(s, axis=1, keepdims=True))
        ec = jnp.exp(s - m)
        fw = jnp.exp(m_w[i] - m)
        inv = 1.0 / (l_w[i] * fw + jnp.sum(ec, axis=1, keepdims=True))
        w_win = (ew[i] * (fw * inv)).astype(jnp.bfloat16)
        w_ctx = (ec * inv).astype(jnp.bfloat16)
        o = jnp.dot(w_win, kvp[band[i], 128:256], preferred_element_type=jnp.float32) + jnp.dot(
            w_ctx, cv, preferred_element_type=jnp.float32
        )
        o = jnp.where(jnp.broadcast_to(lane < HD, (64, 128)), o[0:64], o[64:128])
        attb[tp, i * COLS : (i + 1) * COLS, :] = o.astype(jnp.bfloat16)
        if i % 2 == 1:
            hh = i // 2
            block = attb.at[tp, pl.ds(hh * 128, 128)]
            for t, n in hops:
                send(block, block, as_, apr.at[hh] if n == 3 else ar.at[hh * 3 + n], at(sp, t))

    for hh in range(2):
        rr = pl.ds(hh * 128, 128)
        for n, frm in ((1, left), (2, right), (0, far)):
            block = attb.at[frm, rr]
            arrived(block, ar.at[hh * 3 + n])
            send(block, block, as_, apr.at[hh], at(sp, partner))

    arrived(wfull.at[partner], wr.at[0])
    own_w.wait()
    arrived(wfull.at[pl.ds(0, 2)], wr.at[3])

    for hh in range(2):
        rr = pl.ds(hh * 128, 128)
        arrived(attb.at[pl.ds(0, 2)], apr.at[hh])
        for n in range(HALF // F):
            cols = pl.ds(pl.multiple_of(c * HALF + n * F, F), F)
            acc = jnp.zeros((128, F), jnp.float32)
            for g in range(TP):
                t = jnp.dot(attb[g, rr, :], wfull[g, :, n * F : (n + 1) * F], preferred_element_type=jnp.float32)
                acc = acc + t.astype(jnp.bfloat16).astype(jnp.float32)
            res = latv[rr, cols].astype(jnp.float32) + modf[c * (HALF // F) + n, 4:5, :] * acc
            out[rr, cols] = res.astype(jnp.bfloat16)
            send(out.at[rr, cols], out.at[rr, cols], os_, or_, at(sp, partner))
    arrived(out.at[:, its_half], or_)

    sent(mody, ys)
    sent(modz, zs)
    sent(modf.at[pl.ds(0, TP - 1)], ts)
    sent(cbuf.at[0, 0, pl.ds(0, Z - 1)], czs.at[0])
    sent(cbuf.at[0, 0], czs.at[1])
    sent(cbuf.at[pl.ds(0, 7)], cts)
    sent(ckv.at[pl.ds(0, 3)], cys)
    sent(kvp.at[pl.ds(0, 2 * TOK)], hs)
    sent(wfull.at[pl.ds(0, 7)], ws)
    sent(attb.at[pl.ds(0, 7)], as_)
    sent(out.at[:, my_half], os_)


def per_device(latent, context, cond, cctx, shw, scw, gw, gain, wq, wk, wv, qg, kg, bias, outw):
    hbm = pl.BlockSpec(memory_space=pltpu.HBM)
    vm = pl.BlockSpec(memory_space=pltpu.VMEM)
    bf, f32 = jnp.bfloat16, jnp.float32
    dma = pltpu.SemaphoreType.DMA
    scratch = [
        pltpu.VMEM((2, 1, 16), f32),
        pltpu.VMEM((3, 16, F), bf),
        pltpu.VMEM((1, D), f32),
        pltpu.VMEM((2, 1, HD), f32),
        pltpu.SMEM((15, 2, 31), f32),
        pltpu.VMEM((5, F), f32),
        pltpu.VMEM((Y - 1, 5, F), f32),
        pltpu.VMEM((5, F), f32),
        pltpu.VMEM((Z - 1, 5, F), f32),
        pltpu.VMEM((TP, 5, F), f32),
        pltpu.VMEM((TP, 2, Z, 4, F), bf),
        pltpu.VMEM((128, D), f32),
        pltpu.VMEM((4, 128, 256), bf),
        pltpu.VMEM((TOK, D), f32),
        pltpu.VMEM((TOK, D), bf),
        pltpu.VMEM((128, D), bf),
        pltpu.VMEM((D, 384), bf),
        pltpu.VMEM((TP, 128, HALF), bf),
        pltpu.VMEM((TOK, D), bf),
        pltpu.VMEM((2, 14, COLS, 128), f32),
        pltpu.VMEM((3 * TOK, 256), bf),
        pltpu.VMEM((ROWS, 128, 128), bf),
        pltpu.VMEM((ROWS, 128, 512), f32),
        pltpu.VMEM((TP, TOK, 128), bf),
        pltpu.SemaphoreType.REGULAR,
        dma((5,)),
        dma((4,)),
    ]
    one = dma
    scratch += [one] * 6
    scratch += [dma((2,)), dma((2,)), one, dma((4,)), one, one, dma((2,))]
    scratch += [one, one, one, dma((4,))]
    scratch += [one, dma((6,)), dma((2,)), one, one]
    return pl.pallas_call(
        kernel,
        out_shape=jax.ShapeDtypeStruct((TOK, D), bf),
        in_specs=[hbm] * 15,
        out_specs=vm,
        scratch_shapes=scratch,
        compiler_params=pltpu.CompilerParams(
            collective_id=0, has_side_effects=True, vmem_limit_bytes=40 * 1024 * 1024
        ),
        name="fused",
    )(
        *(
            pltpu.with_memory_space_constraint(a, pltpu.HBM)
            for a in (
                latent, context, cond.reshape(1, 16), cctx.reshape(1, 16), shw, scw, gw, gain.reshape(1, D),
                wq, wk, wv, qg.reshape(1, HD), kg.reshape(1, HD), bias.transpose(1, 0, 2), outw,
            )
        )
    )


def solution(mesh):
    placed = (
        P("sp", None), P("sp", None), P("sp"), P("sp"),
        P("sp", "tp"), P("sp", "tp"), P("sp", "tp"), P(),
        P(None, "tp"), P(None, "tp"), P(None, "tp"), P(), P(),
        P("tp", None, None), P("tp", None),
    )
    return jax.shard_map(
        per_device, mesh=mesh, in_specs=placed, out_specs=P("sp", None), check_vma=False
    )
```

time: 65.1 us -> 62.8 us (0.965); the launches traced: 64.9 us -> 61.9 us
  Pallas kernels: 63.9 us -> 60.9 us
    pallas_call x1, Pallas kernels: 63.9 us -> 60.9 us  [per_device(): pl.pallas_call(kernel, out_shape=jax.ShapeDtypeStruct((TOK, D), bf), in_s...]
where the time goes in v3:
time: 62.8 us; the launch traced here: 61.9 us
  Pallas kernels  60.9 us (97%)
  local copies, waits for them, and re-layouts  0.97 us (2%)
    pallas_call x1, Pallas kernels, per_device(): pl.pallas_call(kernel, out_shape=jax.ShapeDtypeStruct((TOK, D), bf), in_s...  60.9 us

profile of v3, /device:TPU:1, one launch (start us, length us, event | category | flops | bytes accessed | tf_op | source)
XLA Modules:
  0.0 61.9 jit_solution(4094718009209556273)
XLA Ops:
  0.0 60.9 %fused.1 = bf16[256,2048]{1,0:T(8,128)(2,1)S(1)} custom-call(bf16[256,2048]{1,0:T(8,128)(2,1)} %latent.1, bf16[4,2048]{1,0:T(4,128)(2,1)} %context.1, f32[1,16]{1,0:T(1,128)} %bitcast.8, f32[1,16]{1,0:T(1,128)} %bitcast.9, bf16[16,256]{1,0:T(8,128)(2,1)} %shw_h.1, bf16[16,256]{1,0:T(8,128)(2,1)} %scw_h.1, bf16[16,256]{1,0:T(8,128)(2,1)} %gw_h.1, ...), custom_call_target="tpu_custom_call" | custom-call | tf_op jit(solution)/shard_map/fused/pallas_call | solution.py:420
  60.9 1.0 %copy.17 = bf16[256,2048]{1,0:T(8,128)(2,1)} copy(bf16[256,2048]{1,0:T(8,128)(2,1)S(1)} %fused.1) | data formatting | bytes 2097152

commit v4 on v3

--- a/solution.py
+++ b/solution.py
@@ -227,12 +227,37 @@
         arrived(cbuf.at[frm], ctr.at[n])
         send(cbuf.at[frm], cbuf.at[frm], cts, cpr, at(sp, partner))
 
+    arrived(cbuf.at[partner], ctr.at[3])
+    arrived(cbuf.at[pl.ds(0, 3)], cpr)
+
+    for j in range(2 * Z):
+        for g in range(TP):
+            cf[4 * j : 4 * j + 4, g * F : (g + 1) * F] = cbuf[g, j % 2, j // 2].astype(jnp.float32)
+
+    def store_ctx(r, v):
+        cf[r, :] = v
+
+    normed(lambda r: cf[r, :], store_ctx, 128, 16)
+
     pltpu.make_async_copy(wall, wall, loc_sem.at[3]).wait()
     pltpu.make_async_copy(qkg, qkg, small_sem.at[4]).wait()
     arrived(modf.at[pl.ds(0, TP - 1)], tr)
     lane = lax.broadcasted_iota(jnp.int32, (1, 128), 1)
     qg2 = jnp.concatenate([qkg[0], qkg[0]], axis=1)
     kg2 = jnp.concatenate([qkg[1], qkg[1]], axis=1)
+
+    for g in range(TP):
+        gs = slice(g * F, (g + 1) * F)
+        chid[:, gs] = (cf[:, gs] * (1.0 + modf[g, 3:4, :]) + modf[g, 1:2, :]).astype(jnp.bfloat16)
+    kv = jnp.dot(chid[...], wall[:, 0:256], preferred_element_type=jnp.float32)
+    ckv[pair, :, 0:128] = head_norm(kv[:, 0:128], kg2).astype(jnp.bfloat16)
+    ckv[pair, :, 128:256] = kv[:, 128:256].astype(jnp.bfloat16)
+    zh = rem(z, 2)
+    zmate = at((z + 1 - 2 * zh) * Y + y, tp)
+    tok_half = pl.ds(pl.multiple_of(zh * 64, 64), 64)
+    own_pair = ckv.at[pair, tok_half]
+    for k in (3, 2, 1):
+        send(own_pair, own_pair, cys, cyr.at[k - 1], at(z * Y + rem(y + k * side + Y, Y), tp))
 
     for n in range(2):
         r = pl.ds(n * 128, 128)
@@ -248,28 +273,6 @@
     send(own_rows, kvp.at[pl.ds(0, TOK)], hs, hr, at(up, tp))
     send(own_rows, kvp.at[pl.ds(2 * TOK, TOK)], hs, hr, at(down, tp))
 
-    arrived(cbuf.at[partner], ctr.at[3])
-    arrived(cbuf.at[pl.ds(0, 3)], cpr)
-
-    for j in range(2 * Z):
-        for g in range(TP):
-            cf[4 * j : 4 * j + 4, g * F : (g + 1) * F] = cbuf[g, j % 2, j // 2].astype(jnp.float32)
-
-    def store_ctx(r, v):
-        cf[r, :] = v
-
-    normed(lambda r: cf[r, :], store_ctx, 128, 16)
-
-    for g in range(TP):
-        gs = slice(g * F, (g + 1) * F)
-        chid[:, gs] = (cf[:, gs] * (1.0 + modf[g, 3:4, :]) + modf[g, 1:2, :]).astype(jnp.bfloat16)
-    kv = jnp.dot(chid[...], wall[:, 0:256], preferred_element_type=jnp.float32)
-    ckv[pair, :, 0:128] = head_norm(kv[:, 0:128], kg2).astype(jnp.bfloat16)
-    ckv[pair, :, 128:256] = kv[:, 128:256].astype(jnp.bfloat16)
-    own_pair = ckv.at[pair]
-    send(own_pair, own_pair, cys, cyr.at[0], at(z * Y + rem(y + side + Y, Y), tp))
-    send(own_pair, own_pair, cys, cyr.at[1], at(z * Y + rem(y + 3 * side + Y, Y), tp))
-
     for n in range(2):
         r = pl.ds(n * 128, 128)
         q = jnp.dot(hid[r, :], wall[:, 256:384], preferred_element_type=jnp.float32)
@@ -290,9 +293,10 @@
     for f in (right, other(right)):
         send(wfull.at[f, hi], wfull.at[f, hi], ws, wr.at[3], at(sp, left))
 
-    near_pair = ckv.at[rem(pair + side + 4, 4)]
-    arrived(near_pair, cyr.at[0])
-    send(near_pair, near_pair, cys, cyr.at[1], at(z * Y + mate, tp))
+    for k, p in ((1, pair + side), (2, pair - side), (3, pair + 2)):
+        got = ckv.at[rem(p + 4, 4), tok_half]
+        arrived(got, cyr.at[k - 1])
+        send(got, got, cys, cyr.at[3], zmate)
 
     arrived(kvp.at[pl.ds(0, 2 * TOK)], hr)
 
@@ -317,7 +321,7 @@
         m_w.append(m)
         l_w.append(jnp.sum(e, axis=1, keepdims=True))
 
-    arrived(ckv.at[pl.ds(0, 2)], cyr.at[1])
+    arrived(ckv.at[pl.ds(0, 3), pl.ds(0, 64)], cyr.at[3])
 
     ck = ckv[:, :, 0:128].reshape(512, 128)
     cv = ckv[:, :, 128:256].reshape(512, 128)
@@ -414,7 +418,7 @@
     ]
     one = dma
     scratch += [one] * 6
-    scratch += [dma((2,)), dma((2,)), one, dma((4,)), one, one, dma((2,))]
+    scratch += [dma((2,)), dma((2,)), one, dma((4,)), one, one, dma((4,))]
     scratch += [one, one, one, dma((4,))]
     scratch += [one, dma((6,)), dma((2,)), one, one]
     return pl.pallas_call(

time: 62.8 us -> 64.7 us (1.030); the launches traced: 61.9 us -> 64.6 us
  Pallas kernels: 60.9 us -> 63.6 us
    pallas_call x1, Pallas kernels: 60.9 us -> 63.6 us  [per_device(): pl.pallas_call(kernel, out_shape=jax.ShapeDtypeStruct((TOK, D), bf), in_s...]
where the time goes in v4:
time: 64.7 us; the launch traced here: 64.6 us
  Pallas kernels  63.6 us (98%)
  local copies, waits for them, and re-layouts  0.97 us (1%)
    pallas_call x1, Pallas kernels, per_device(): pl.pallas_call(kernel, out_shape=jax.ShapeDtypeStruct((TOK, D), bf), in_s...  63.6 us

profile of v4, /device:TPU:1, one launch (start us, length us, event | category | flops | bytes accessed | tf_op | source)
XLA Modules:
  0.0 64.6 jit_solution(17530989487293424583)
XLA Ops:
  0.0 63.6 %fused.1 = bf16[256,2048]{1,0:T(8,128)(2,1)S(1)} custom-call(bf16[256,2048]{1,0:T(8,128)(2,1)} %latent.1, bf16[4,2048]{1,0:T(4,128)(2,1)} %context.1, f32[1,16]{1,0:T(1,128)} %bitcast.8, f32[1,16]{1,0:T(1,128)} %bitcast.9, bf16[16,256]{1,0:T(8,128)(2,1)} %shw_h.1, bf16[16,256]{1,0:T(8,128)(2,1)} %scw_h.1, bf16[16,256]{1,0:T(8,128)(2,1)} %gw_h.1, ...), custom_call_target="tpu_custom_call" | custom-call | tf_op jit(solution)/shard_map/fused/pallas_call | solution.py:424
  63.6 1.0 %copy.17 = bf16[256,2048]{1,0:T(8,128)(2,1)} copy(bf16[256,2048]{1,0:T(8,128)(2,1)S(1)} %fused.1) | data formatting | bytes 2097152

commit v5 on v4

--- a/solution.py
+++ b/solution.py
@@ -54,10 +54,10 @@
     y = rem(sp, Y)
     z = lax.div(sp, jnp.int32(Y))
     c = rem(tp, 2)
-    odd = rem(y, 2)
-    mate = y + 1 - 2 * odd
+    odd = rem(y + 1, 2)
+    mate = rem(y + Y + 1 - 2 * odd, Y)
     side = 2 * odd - 1
-    pair = lax.div(y, jnp.int32(2))
+    pair = rem(lax.div(y + 1, jnp.int32(2)), 4)
     partner = tp + 1 - 2 * c
     up = rem(sp + 1, SP)
     down = rem(sp + SP - 1, SP)

time: 64.7 us -> 62.1 us (0.960)
  Pallas kernels: 63.6 us -> 61 us
    pallas_call x1, Pallas kernels: 63.6 us -> 61 us  [per_device(): pl.pallas_call(kernel, out_shape=jax.ShapeDtypeStruct((TOK, D), bf), in_s...]
where the time goes in v5:
time: 62.1 us; the launch traced here: 61.9 us
  Pallas kernels  61 us (98%)
  local copies, waits for them, and re-layouts  0.97 us (2%)
    pallas_call x1, Pallas kernels, per_device(): pl.pallas_call(kernel, out_shape=jax.ShapeDtypeStruct((TOK, D), bf), in_s...  61 us

profile of v5, /device:TPU:1, one launch (start us, length us, event | category | flops | bytes accessed | tf_op | source)
XLA Modules:
  0.0 61.9 jit_solution(16542968189471681231)
XLA Ops:
  0.0 61.0 %fused.1 = bf16[256,2048]{1,0:T(8,128)(2,1)S(1)} custom-call(bf16[256,2048]{1,0:T(8,128)(2,1)} %latent.1, bf16[4,2048]{1,0:T(4,128)(2,1)} %context.1, f32[1,16]{1,0:T(1,128)} %bitcast.8, f32[1,16]{1,0:T(1,128)} %bitcast.9, bf16[16,256]{1,0:T(8,128)(2,1)} %shw_h.1, bf16[16,256]{1,0:T(8,128)(2,1)} %scw_h.1, bf16[16,256]{1,0:T(8,128)(2,1)} %gw_h.1, ...), custom_call_target="tpu_custom_call" | custom-call | tf_op jit(solution)/shard_map/fused/pallas_call | solution.py:424
  61.0 1.0 %copy.17 = bf16[256,2048]{1,0:T(8,128)(2,1)} copy(bf16[256,2048]{1,0:T(8,128)(2,1)S(1)} %fused.1) | data formatting | bytes 2097152

commit v6 on v5

--- a/solution.py
+++ b/solution.py
@@ -223,16 +223,23 @@
     for k in (4, 3, 5, 2, 6, 1, 7):
         send(modf.at[tp], modf.at[tp], ts, tr, t_peer(k))
 
+    def unpack(g):
+        cols = pl.ds(pl.multiple_of(g * F, F), F)
+        for j in range(2 * Z):
+            cf[4 * j : 4 * j + 4, cols] = cbuf[g, j % 2, j // 2].astype(jnp.float32)
+
+    unpack(tp)
     for n, frm in ((1, left), (2, right), (0, far)):
         arrived(cbuf.at[frm], ctr.at[n])
         send(cbuf.at[frm], cbuf.at[frm], cts, cpr, at(sp, partner))
-
+        if n:
+            unpack(frm)
+    unpack(far)
     arrived(cbuf.at[partner], ctr.at[3])
+    unpack(partner)
     arrived(cbuf.at[pl.ds(0, 3)], cpr)
-
-    for j in range(2 * Z):
-        for g in range(TP):
-            cf[4 * j : 4 * j + 4, g * F : (g + 1) * F] = cbuf[g, j % 2, j // 2].astype(jnp.float32)
+    for frm in (left, right, far):
+        unpack(other(frm))
 
     def store_ctx(r, v):
         cf[r, :] = v
@@ -325,24 +332,28 @@
 
     ck = ckv[:, :, 0:128].reshape(512, 128)
     cv = ckv[:, :, 128:256].reshape(512, 128)
-    for i in range(ROWS):
-        s = lax.dot_general(q2[i], ck, nt, preferred_element_type=jnp.float32)
-        m = jnp.maximum(m_w[i], jnp.max(s, axis=1, keepdims=True))
-        ec = jnp.exp(s - m)
-        fw = jnp.exp(m_w[i] - m)
-        inv = 1.0 / (l_w[i] * fw + jnp.sum(ec, axis=1, keepdims=True))
-        w_win = (ew[i] * (fw * inv)).astype(jnp.bfloat16)
-        w_ctx = (ec * inv).astype(jnp.bfloat16)
-        o = jnp.dot(w_win, kvp[band[i], 128:256], preferred_element_type=jnp.float32) + jnp.dot(
-            w_ctx, cv, preferred_element_type=jnp.float32
+    for hh in range(2):
+        two = range(2 * hh, 2 * hh + 2)
+        s = lax.dot_general(
+            q2[2 * hh : 2 * hh + 2].reshape(256, 128), ck, nt, preferred_element_type=jnp.float32
         )
-        o = jnp.where(jnp.broadcast_to(lane < HD, (64, 128)), o[0:64], o[64:128])
-        attb[tp, i * COLS : (i + 1) * COLS, :] = o.astype(jnp.bfloat16)
-        if i % 2 == 1:
-            hh = i // 2
-            block = attb.at[tp, pl.ds(hh * 128, 128)]
-            for t, n in hops:
-                send(block, block, as_, apr.at[hh] if n == 3 else ar.at[hh * 3 + n], at(sp, t))
+        mw = jnp.concatenate([m_w[i] for i in two], axis=0)
+        lw = jnp.concatenate([l_w[i] for i in two], axis=0)
+        m = jnp.maximum(mw, jnp.max(s, axis=1, keepdims=True))
+        e = jnp.exp(s - m)
+        fw = jnp.exp(mw - m)
+        inv = 1.0 / (lw * fw + jnp.sum(e, axis=1, keepdims=True))
+        o_ctx = jnp.dot((e * inv).astype(jnp.bfloat16), cv, preferred_element_type=jnp.float32)
+        fi = fw * inv
+        for j, i in enumerate(two):
+            w_win = (ew[i] * fi[j * 128 : (j + 1) * 128]).astype(jnp.bfloat16)
+            o = jnp.dot(w_win, kvp[band[i], 128:256], preferred_element_type=jnp.float32)
+            o = o + o_ctx[j * 128 : (j + 1) * 128]
+            o = jnp.where(jnp.broadcast_to(lane < HD, (64, 128)), o[0:64], o[64:128])
+            attb[tp, i * COLS : (i + 1) * COLS, :] = o.astype(jnp.bfloat16)
+        block = attb.at[tp, pl.ds(hh * 128, 128)]
+        for t, n in hops:
+            send(block, block, as_, apr.at[hh] if n == 3 else ar.at[hh * 3 + n], at(sp, t))
 
     for hh in range(2):
         rr = pl.ds(hh * 128, 128)

time: 62.1 us -> 61.5 us (level)
  no operation moved by 1% of the time
where the time goes in v6:
time: 61.5 us; the launch traced here: 61.4 us
  Pallas kernels  60.4 us (98%)
  local copies, waits for them, and re-layouts  0.97 us (2%)
    pallas_call x1, Pallas kernels, per_device(): pl.pallas_call(kernel, out_shape=jax.ShapeDtypeStruct((TOK, D), bf), in_s...  60.4 us

profile of v6, /device:TPU:1, one launch (start us, length us, event | category | flops | bytes accessed | tf_op | source)
XLA Modules:
  0.0 61.4 jit_solution(13231903189970983059)
XLA Ops:
  0.0 60.4 %fused.1 = bf16[256,2048]{1,0:T(8,128)(2,1)S(1)} custom-call(bf16[256,2048]{1,0:T(8,128)(2,1)} %latent.1, bf16[4,2048]{1,0:T(4,128)(2,1)} %context.1, f32[1,16]{1,0:T(1,128)} %bitcast.8, f32[1,16]{1,0:T(1,128)} %bitcast.9, bf16[16,256]{1,0:T(8,128)(2,1)} %shw_h.1, bf16[16,256]{1,0:T(8,128)(2,1)} %scw_h.1, bf16[16,256]{1,0:T(8,128)(2,1)} %gw_h.1, ...), custom_call_target="tpu_custom_call" | custom-call | tf_op jit(solution)/shard_map/fused/pallas_call | solution.py:435
  60.4 1.0 %copy.17 = bf16[256,2048]{1,0:T(8,128)(2,1)} copy(bf16[256,2048]{1,0:T(8,128)(2,1)S(1)} %fused.1) | data formatting | bytes 2097152
